TPU v7x, 32 devices: a whole 2x2x4 slice. The times are simulated.
32 devices in a mesh: sp: 4 (over z), tp: 8 (over y, x, core).
Axes of the slice: x: 2, y: 2, z: 4, core: 2. Of those that a mesh axis runs over, the one named last changes fastest.
Arguments:
- token_values: bfloat16 [1024, 2048], P('sp', 'tp'), may hold values from -6 to 6
- write_keys: bfloat16 [1024, 1024], P('sp', 'tp'), may hold values from -0.4375 to 0.4375
- read_keys: bfloat16 [1024, 1024], P('sp', 'tp'), may hold values from -0.4375 to 0.4375
- log_decay: float32 [32, 1024], P('tp', 'sp'), may hold values from -0.7 to 0, as said below
- out_gate: bfloat16 [1024, 2048], P('sp', 'tp'), may hold values from -6 to 6
- out_proj: bfloat16 [4096, 2048], P(None, 'tp'), may hold values from -0.125 to 0.125
- mixed: bfloat16 [1024, 4096], P('sp'), may hold values from -6 to 6
- cotangent: bfloat16 [1024, 4096], P('sp'), may hold values from -8 to 8
- route_ids: int32 [1024, 2], P('sp'), may hold values from 0 to 3, all different within a row; in each aligned block of 256 rows (0 to 255, 256 to 511, ...) at most 192 rows name the same one
- route_weights: float32 [1024, 2], P('sp'), may hold values from 0.25 to 1
- w_gate: bfloat16 [4, 4096, 2048], P('sp', None, 'tp'), may hold values from -0.09375 to 0.09375
- w_up: bfloat16 [4, 4096, 2048], P('sp', None, 'tp'), may hold values from -0.09375 to 0.09375
- w_down: bfloat16 [4, 2048, 4096], P('sp', 'tp'), may hold values from -0.125 to 0.125
Outputs:
- value_grad: bfloat16 [1024, 2048], P('sp', 'tp')
- write_grad: bfloat16 [1024, 1024], P('sp', 'tp')
- read_grad: bfloat16 [1024, 1024], P('sp', 'tp')
- gate_grad: bfloat16 [1024, 2048], P('sp', 'tp')
- proj_grad: float32 [4096, 2048], P('sp', 'tp')
- gate_weight_grad: bfloat16 [4, 4096, 2048], P('sp', None, 'tp')
- up_weight_grad: bfloat16 [4, 4096, 2048], P('sp', None, 'tp')
- down_weight_grad: bfloat16 [4, 2048, 4096], P('sp', 'tp')
Inputs may be any that keep to these rules, and one draw needn't show every extreme that they name: `route_ids`: each row names 2 different experts. Within the rows of one device no expert is named more than 192 times, and in every draw some expert is named exactly 192 times by the rows of some device. `log_decay`: every entry is negative.
All inputs are finite; a program needn't handle non-finite values.
Results may differ from a plain program's by a relative error of at most 0.019.
Values may be sent and summed in bfloat16 or wider, within the bound.
A program may use at most 128 MiB of HBM per device.

v0:
```python
import functools

import jax
import jax.numpy as jnp
from jax import lax
from jax.experimental import pallas as pl
from jax.experimental.pallas import tpu as pltpu
from jax.sharding import PartitionSpec as P

HEAD_DIM = 64
STATE = 128

F32 = jnp.float32
BF16 = jnp.bfloat16


def dot(a, b, ca=1, cb=0):
    return lax.dot_general(a, b, (((ca,), (cb,)), ((), ())), preferred_element_type=F32)


def shift(x, by):
    n = lax.axis_size("sp")
    return lax.ppermute(x, "sp", [(i, (i + by) % n) for i in range(n)])


def spread_kernel(n, arrays, far, *refs):
    sends, outs = refs[:arrays], refs[arrays : 2 * arrays]
    send_sem, recv_sem, local_sem = refs[2 * arrays :]
    t = lax.axis_index("tp")
    s = lax.axis_index("sp")
    blocks, rows, cols = sends[0].shape
    half = rows // 2
    chunks = [(a, j) for a in range(arrays) for j in range(blocks)]
    near = [{"tp": t ^ bit} for bit in (1, 2, 4)]
    other, across, along = near
    peers = list(near)
    if far:
        peers += [{"sp": lax.rem(s + j, n)} for j in range(1, n)]
    barrier = pltpu.get_barrier_semaphore()
    for peer in peers:
        pl.semaphore_signal(barrier, inc=1, device_id=peer, device_id_type=pl.DeviceIdType.MESH)
    pl.semaphore_wait(barrier, len(peers))

    def window(c, bits, start=0, count=rows):
        a, j = chunks[c]
        at = pl.multiple_of((t ^ bits) * cols, 128)
        return outs[a].at[j, pl.ds(start, count), pl.ds(at, cols)]

    def copy(c, kind, src, dst, device):
        return pltpu.make_async_remote_copy(
            src_ref=src,
            dst_ref=dst,
            send_sem=send_sem.at[c, kind],
            recv_sem=recv_sem.at[c, kind],
            device_id=device,
            device_id_type=pl.DeviceIdType.MESH,
        )

    started = []

    def start(*args):
        made = copy(*args)
        made.start()
        started.append(made)

    def arrived(c, kind, dst, device):
        copy(c, kind, dst, dst, device).wait_recv()

    locals_ = []
    for c, (a, j) in enumerate(chunks):
        if far:
            start(c, 0, sends[a].at[j], window(c, 0), {"sp": lax.rem(s + j + 1, n)})
        else:
            made = pltpu.make_async_copy(sends[a].at[j], window(c, 0), local_sem.at[c])
            made.start()
            locals_.append(made)
    total = len(chunks)
    for k in range(total + 2):
        if k < total:
            if far:
                arrived(k, 0, window(k, 0), {"sp": lax.rem(s + 1, n)})
                own = window(k, 0)
            else:
                own = sends[chunks[k][0]].at[chunks[k][1]]
            start(k, 1, own, window(k, 0), across)
            start(k, 2, own, window(k, 0), along)
            start(k, 5, own, window(k, 0), other)
        c = k - 1
        if 0 <= c < total:
            arrived(c, 1, window(c, 2), across)
            start(c, 3, window(c, 2, 0, half), window(c, 2, 0, half), along)
            start(c, 6, window(c, 2), window(c, 2), other)
            arrived(c, 2, window(c, 4), along)
            start(c, 4, window(c, 4, half, rows - half), window(c, 4, half, rows - half), across)
            start(c, 7, window(c, 4), window(c, 4), other)
        c = k - 2
        if 0 <= c < total:
            arrived(c, 3, window(c, 6, 0, half), along)
            arrived(c, 4, window(c, 6, half, rows - half), across)
            start(c, 8, window(c, 6), window(c, 6), other)
    for c in range(total):
        for kind, bits in ((5, 1), (6, 3), (7, 5), (8, 7)):
            arrived(c, kind, window(c, bits), other)
    for made in started:
        made.wait_send()
    for made in locals_:
        made.wait()


def spread(arrays, far, collective_id):
    n = lax.axis_size("sp")
    ranks = lax.axis_size("tp")
    blocks, rows, cols = arrays[0].shape
    count = len(arrays)
    total = count * blocks
    space = pl.ANY if far else pltpu.VMEM
    got = pl.pallas_call(
        functools.partial(spread_kernel, n, count, far),
        out_shape=[jax.ShapeDtypeStruct((blocks, rows, ranks * cols), BF16)] * count,
        in_specs=[pl.BlockSpec(memory_space=space)] * count,
        out_specs=[pl.BlockSpec(memory_space=pl.ANY)] * count,
        scratch_shapes=[
            pltpu.SemaphoreType.DMA((total, 9)),
            pltpu.SemaphoreType.DMA((total, 9)),
            pltpu.SemaphoreType.DMA((total,)),
        ],
        compiler_params=pltpu.CompilerParams(collective_id=collective_id, has_side_effects=True),
    )(*arrays)
    return [g.reshape(blocks * rows, ranks * cols) for g in got]


def body(
    token_values,
    write_keys,
    read_keys,
    log_decay,
    out_gate,
    out_proj,
    mixed,
    cotangent,
    route_ids,
    route_weights,
    w_gate,
    w_up,
    w_down,
):
    tok, width = mixed.shape
    n = lax.axis_size("sp")
    cap = 3 * tok // n
    share = width // lax.axis_size("tp")
    own = lax.axis_index("sp")
    offset = lax.axis_index("tp") * share

    rel = lax.rem(route_ids - own + n, n)
    hit = rel[:, :, None] == jnp.arange(n, dtype=jnp.int32)[None, None, :]
    member = jnp.any(hit, axis=1)
    weight = jnp.sum(jnp.where(hit, route_weights[:, :, None], 0.0), axis=1)
    order = jnp.arange(tok, dtype=jnp.int32)
    before = (order[:, None] > order[None, :]).astype(BF16)
    slot = dot(before, member.astype(BF16)).astype(jnp.int32)
    slot = jnp.where(member, slot, -1).T
    place = jnp.arange(cap, dtype=jnp.int32)
    chosen = slot[:, None, :] == place[None, :, None]
    onehot = chosen.astype(BF16)
    row_weight = jnp.sum(jnp.where(chosen, weight.T[:, None, :], 0.0), axis=2)

    mixed_part = lax.dynamic_slice_in_dim(mixed, offset, share, 1)
    cot_part = lax.dynamic_slice_in_dim(cotangent, offset, share, 1)
    away = onehot[1:].reshape((n - 1) * cap, tok)
    away_weight = row_weight[1:].reshape((n - 1) * cap, 1)
    send_rows = dot(away, mixed_part).astype(BF16).reshape(n - 1, cap, share)
    send_scaled = (dot(away, cot_part) * away_weight).astype(BF16).reshape(n - 1, cap, share)
    rem_rows, rem_scaled = spread([send_rows, send_scaled], True, 1)
    loc_rows = dot(onehot[0], mixed).astype(BF16)
    loc_scaled = (dot(onehot[0], cotangent) * row_weight[0][:, None]).astype(BF16)

    heads = log_decay.shape[0]
    groups = write_keys.shape[1] // STATE
    per_group = heads // groups
    cumul = jnp.cumsum(log_decay, axis=1)
    total = cumul[:, -1]
    tails = jnp.exp(total[:, None] - cumul)
    leads = jnp.exp(cumul)
    values = token_values.astype(F32)
    gate = out_gate.astype(F32)
    sig = jax.nn.sigmoid(gate)
    silu = gate * sig
    causal = order[:, None] >= order[None, :]

    def widen(per_head):
        return jnp.repeat(per_head.T, HEAD_DIM, axis=1)

    tails_wide = widen(tails)
    leads_wide = widen(leads)
    tailed = (values * tails_wide).astype(BF16)

    def cols(a, g):
        k = per_group * HEAD_DIM
        return a[:, g * k : (g + 1) * k]

    def keys(a, g):
        return a[:, g * STATE : (g + 1) * STATE]

    def head(a, h):
        return a[:, h * HEAD_DIM : (h + 1) * HEAD_DIM]

    local_end = jnp.concatenate(
        [dot(cols(tailed, g), keys(write_keys, g), 0, 0) for g in range(groups)], axis=0
    )
    packed = jnp.concatenate(
        [local_end, jnp.broadcast_to(total[:, None], (heads, STATE))], axis=0
    ).astype(BF16)
    lengths = heads * HEAD_DIM
    entering = jnp.zeros((lengths, STATE), F32)
    run = jnp.zeros((heads,), F32)
    for j in range(1, n):
        got = shift(packed, j).astype(F32)
        live = own >= j
        factor = jnp.where(live, jnp.exp(run), 0.0)
        entering = entering + jnp.repeat(factor, HEAD_DIM)[:, None] * got[:lengths]
        run = run + jnp.where(live, got[lengths:, 0], 0.0)
    ahead = [shift(packed[lengths:], -j).astype(F32)[:, 0] for j in range(1, n)]
    entering_b = entering.astype(BF16)

    decay_of, kept, outs = [], [], []
    scores = [dot(keys(read_keys, g), keys(write_keys, g), 1, 1) for g in range(groups)]
    for h in range(heads):
        span = cumul[h][:, None] - cumul[h][None, :]
        decay = jnp.exp(jnp.where(causal, span, -jnp.inf))
        decay_of.append(decay)
        kept.append((scores[h // per_group] * decay).astype(BF16))
        outs.append(dot(kept[h], head(token_values, h)))
    carried = jnp.concatenate(
        [
            dot(keys(read_keys, g), entering_b[g * per_group * HEAD_DIM : (g + 1) * per_group * HEAD_DIM], 1, 1)
            for g in range(groups)
        ],
        axis=1,
    )
    y = jnp.concatenate(outs, axis=1) + carried * leads_wide
    gated_b = (y * silu).astype(BF16)

    def both(loc, rem, w, cb):
        return jnp.concatenate([dot(loc, w, 1, cb), dot(rem, w, 1, cb)], axis=0)

    def over_rows(loc, rem, d):
        return (dot(loc, d[:cap], 0, 0) + dot(rem, d[cap:], 0, 0)).astype(BF16)

    gate_pre = both(loc_rows, rem_rows, w_gate[0], 0)
    up_pre = both(loc_rows, rem_rows, w_up[0], 0)
    sigma = jax.nn.sigmoid(gate_pre)
    act_gate = gate_pre * sigma
    hidden = (act_gate * up_pre).astype(BF16)
    d_hidden = both(loc_scaled, rem_scaled, w_down[0], 1)
    d_gate = (d_hidden * up_pre * sigma * (1.0 + gate_pre * (1.0 - sigma))).astype(BF16)
    d_up = (d_hidden * act_gate).astype(BF16)
    portion = (dot(d_gate, w_gate[0], 1, 1) + dot(d_up, w_up[0], 1, 1)).astype(BF16)
    summed = lax.psum_scatter(portion, "tp", scatter_dimension=1, tiled=True)
    grad_gate = over_rows(loc_rows, rem_rows, d_gate)
    grad_up = over_rows(loc_rows, rem_rows, d_up)
    grad_down = (
        dot(hidden[:cap], loc_scaled, 0, 0) + dot(hidden[cap:], rem_scaled, 0, 0)
    ).astype(BF16)

    came = [summed[:cap]] + [
        shift(summed[j * cap : (j + 1) * cap], -j) for j in range(1, n)
    ]
    came = jnp.concatenate(came, axis=0)
    back = dot(onehot.reshape(n * cap, tok), came, 0, 0)
    grad_part = (cot_part.astype(F32) + back).astype(BF16)
    (grad_mixed,) = spread([grad_part.reshape(2, tok // 2, share)], False, 2)

    out_grad = dot(grad_mixed, out_proj)
    quarter = width // n
    piece = quarter // lax.axis_size("tp")
    lane = lax.axis_index("tp") * piece
    if piece % 128 == 0:
        send_mixed = jnp.stack(
            [
                lax.dynamic_slice_in_dim(grad_mixed, lax.rem(own + j, n) * quarter + lane, piece, 1)
                for j in range(1, n)
            ]
        )
        (far_mixed,) = spread([send_mixed], True, 3)
        own_mixed = lax.dynamic_slice_in_dim(grad_mixed, own * quarter, quarter, 1)
        far_gated = jnp.concatenate([shift(gated_b, j) for j in range(1, n)], axis=0)
        proj_grad = dot(own_mixed, gated_b, 0, 0) + dot(far_mixed, far_gated, 0, 0)
    else:
        proj_part = dot(grad_mixed, gated_b, 0, 0).astype(BF16)
        proj_grad = lax.psum_scatter(proj_part, "sp", scatter_dimension=0, tiled=True).astype(F32)

    outer = out_grad * silu
    outer_b = outer.astype(BF16)
    led = (outer * leads_wide).astype(BF16)
    local_back = jnp.concatenate(
        [dot(cols(led, g), keys(read_keys, g), 0, 0) for g in range(groups)], axis=0
    ).astype(BF16)
    leaving = jnp.zeros((lengths, STATE), F32)
    run = jnp.zeros((heads,), F32)
    for j in range(1, n):
        got = shift(local_back, -j).astype(F32)
        live = own + j < n
        factor = jnp.where(live, jnp.exp(run), 0.0)
        leaving = leaving + jnp.repeat(factor, HEAD_DIM)[:, None] * got
        run = run + jnp.where(live, ahead[j - 1], 0.0)
    leaving_b = leaving.astype(BF16)

    d_values, d_writes, d_reads = [], [], []
    for g in range(groups):
        d_scores = 0.0
        for r in range(per_group):
            h = g * per_group + r
            d_scores = d_scores + dot(head(outer_b, h), head(token_values, h), 1, 1) * decay_of[h]
            d_values.append(dot(kept[h], head(outer_b, h), 0, 0))
        d_scores = d_scores.astype(BF16)
        span = slice(g * per_group * HEAD_DIM, (g + 1) * per_group * HEAD_DIM)
        d_reads.append(dot(d_scores, keys(write_keys, g)) + dot(led[:, span], entering_b[span]))
        d_writes.append(
            dot(d_scores, keys(read_keys, g), 0, 0) + dot(tailed[:, span], leaving_b[span])
        )
    from_end = jnp.concatenate(
        [
            dot(keys(write_keys, g), leaving_b[g * per_group * HEAD_DIM : (g + 1) * per_group * HEAD_DIM], 1, 1)
            for g in range(groups)
        ],
        axis=1,
    )
    d_values = jnp.concatenate(d_values, axis=1) + from_end * tails_wide
    d_out_gate = out_grad * y * sig * (1.0 + gate * (1.0 - sig))
    return (
        d_values.astype(BF16),
        jnp.concatenate(d_writes, axis=1).astype(BF16),
        jnp.concatenate(d_reads, axis=1).astype(BF16),
        d_out_gate.astype(BF16),
        proj_grad,
        grad_gate[None],
        grad_up[None],
        grad_down[None],
    )


def solution(mesh):
    return jax.shard_map(
        body,
        mesh=mesh,
        in_specs=(
            P("sp", "tp"),
            P("sp", "tp"),
            P("sp", "tp"),
            P("tp", "sp"),
            P("sp", "tp"),
            P(None, "tp"),
            P("sp", None),
            P("sp", None),
            P("sp", None),
            P("sp", None),
            P("sp", None, "tp"),
            P("sp", None, "tp"),
            P("sp", "tp", None),
        ),
        out_specs=(
            P("sp", "tp"),
            P("sp", "tp"),
            P("sp", "tp"),
            P("sp", "tp"),
            P("sp", "tp"),
            P("sp", None, "tp"),
            P("sp", None, "tp"),
            P("sp", "tp", None),
        ),
        check_vma=False,
    )
```

profile of v0, /device:TPU:0, one launch (start us, length us, event | category | flops | bytes accessed | tf_op | source)
XLA Modules:
  0.0 257.1 jit_solution(7609990974686661867)
XLA Ops:
  9.5 3.3 %convolution_convert_fusion = bf16[192,4096]{1,0:T(8,128)(2,1)} fusion(bf16[256,4096]{1,0:T(8,128)(2,1)} %param.19, pred[4,192,256]{2,1,0:T(32,128)(4,1)S(1)} %iota_compare_fusion), kind=kOutput, calls=%fused_computation.9 | convolution fusion | flops 403439616 | bytes 3719168 | tf_op jit(solution)/shard_map/dot_general | solution.py:18
  12.9 2.1 convolution_convert_fusion.1
  15.0 2.1 fusion.22
  17.1 59.9 %shard_map.188 = (bf16[3,192,4096]{2,1,0:T(8,128)(2,1)}, bf16[3,192,4096]{2,1,0:T(8,128)(2,1)}) custom-call(bf16[3,192,512]{2,1,0:T(8,128)(2,1)} %bitcast.143, bf16[3,192,512]{2,1,0:T(8,128)(2,1)} %bitcast.144), custom_call_target="tpu_custom_call" | custom-call | tf_op jit(solution)/shard_map/pallas_call | solution.py:117
  76.9 4.5 %fusion.14 = f32[576,256]{1,0:T(8,128)S(1)} fusion(bf16[576,4096]{1,0:T(8,128)(2,1)} %bitcast.155, bf16[1,4096,256]{2,1,0:T(8,128)(2,1)} %param.24), kind=kOutput, calls=%fused_computation.20 | convolution fusion | flops 1207959552 | bytes 7405568 | tf_op jit(solution)/shard_map/dot_general | solution.py:18
  92.0 5.7 %add_convert_fusion = bf16[768,4096]{1,0:T(8,128)(2,1)} fusion(f32[768,4096]{1,0:T(8,128)S(1)} %fusion.7, bf16[768,256]{1,0:T(8,128)(2,1)} %get-tuple-element.45, bf16[1,4096,256]{2,1,0:T(8,128)(2,1)S(1)} %copy-done.6), kind=kOutput, calls=%fused_computation | convolution fusion | flops 1616904192 | bytes 21364736 | tf_op jit(solution)/shard_map/dot_general | solution.py:18
  100.7 6.3 %collective-permute-start.8 = (bf16[260,128]{1,0:T(8,128)(2,1)S(1)}, bf16[260,128]{1,0:T(8,128)(2,1)S(1)}, u32[]{:S(2)}, u32[]{:S(2)}) collective-permute-start(bf16[260,128]{1,0:T(8,128)(2,1)S(1)} %pad_maximum_fusion.4), channel_id=1, source_target_pairs={{0,8},{8,16},{16,24},{24,0},{1,9},{9,17},{17,25},{25,1},{2,10},{10... | collective-permute-start | bytes 199688 | tf_op jit(solution)/shard_map/ppermute | solution.py:23
  109.5 1.9 collective-permute-start.4
  116.4 4.5 %fusion.51 = f32[256,4096]{1,0:T(8,128)S(1)} fusion(bf16[576,4096]{1,0:T(8,128)(2,1)} %bitcast.139, bf16[768,256]{1,0:T(8,128)(2,1)S(1)} %get-tuple-element.43), kind=kOutput, calls=%fused_computation.87 | convolution fusion | flops 1207959552 | bytes 9207808 | tf_op jit(solution)/shard_map/dot_general | solution.py:18
  121.0 2.1 fusion.4
  125.0 2.1 fusion.5
  129.0 2.1 fusion.6
  133.8 30.1 %reduce-scatter.2.cloned.1.call-done = bf16[768,512]{1,0:T(8,128)(2,1)} async-done(((bf16[768,4096]{1,0:T(8,128)(2,1)}), bf16[768,512]{1,0:T(8,128)(2,1)}) %reduce-scatter.2.cloned.1.call-update) | async-done | bytes 786448 | tf_op jit(solution)/shard_map/reduce_scatter | solution.py:258
  165.2 3.4 %collective-permute-start = (bf16[192,512]{1,0:T(8,128)(2,1)S(1)}, bf16[192,512]{1,0:T(8,128)(2,1)S(1)}, u32[]{:S(2)}, u32[]{:S(2)}) collective-permute-start(bf16[192,512]{1,0:T(8,128)(2,1)S(1)} %get-tuple-element.49), channel_id=1, source_target_pairs={{0,24},{8,0},{16,8},{24,16},{1,25},{9,1},{17,9},{25,17},{2,26},{10... | collective-permute-start | bytes 589832 | tf_op jit(solution)/shard_map/ppermute | solution.py:23
  170.7 3.2 %collective-permute-done = bf16[192,512]{1,0:T(8,128)(2,1)S(1)} collective-permute-done((bf16[192,512]{1,0:T(8,128)(2,1)S(1)}, bf16[192,512]{1,0:T(8,128)(2,1)S(1)}, u32[]{:S(2)}, u32[]{:S(2)}) %collective-permute-start) | collective-permute-done | bytes 196640 | tf_op jit(solution)/shard_map/ppermute | solution.py:23
  173.9 11.4 %collective-permute-done.1 = bf16[192,512]{1,0:T(8,128)(2,1)S(1)} collective-permute-done((bf16[192,512]{1,0:T(8,128)(2,1)S(1)}, bf16[192,512]{1,0:T(8,128)(2,1)S(1)}, u32[]{:S(2)}, u32[]{:S(2)}) %collective-permute-start.1) | collective-permute-done | bytes 196640 | tf_op jit(solution)/shard_map/ppermute | solution.py:23
  185.3 2.3 fusion.23
  187.6 15.0 %shard_map.189 = bf16[2,128,4096]{2,1,0:T(8,128)(2,1)} custom-call(bf16[2,128,512]{2,1,0:T(8,128)(2,1)} %bitcast.149), custom_call_target="tpu_custom_call" | custom-call | tf_op jit(solution)/shard_map/pallas_call | solution.py:117
  202.7 2.6 %fusion.110 = f32[256,256]{0,1:T(8,128)S(1)} fusion(bf16[256,4096]{1,0:T(8,128)(2,1)} %bitcast.136, bf16[4096,256]{1,0:T(8,128)(2,1)S(1)} %copy-done.8), kind=kOutput, calls=%fused_computation.186 | convolution fusion | flops 536870912 | bytes 4456448 | tf_op jit(solution)/shard_map/dot_general | solution.py:18
  206.8 2.0 collective-permute-start.12
  210.4 2.9 %collective-permute-start.3 = (bf16[256,128]{1,0:T(8,128)(2,1)S(1)}, bf16[256,128]{1,0:T(8,128)(2,1)S(1)}, u32[]{:S(2)}, u32[]{:S(2)}) collective-permute-start(bf16[256,128]{1,0:T(8,128)(2,1)S(1)} %convolution_convert_fusion.3), channel_id=1, source_target_pairs={{0,24},{8,0},{16,8},{24,16},{1,25},{9,1},{17,9},{25,17},{2,26},{10... | collective-permute-start | bytes 196616 | tf_op jit(solution)/shard_map/ppermute | solution.py:23
  218.8 21.3 %shard_map.190 = bf16[3,256,1024]{2,1,0:T(8,128)(2,1)} custom-call(bf16[3,256,128]{2,1,0:T(8,128)(2,1)} %pad_maximum_fusion.3.refs_0_), custom_call_target="tpu_custom_call" | custom-call | tf_op jit(solution)/shard_map/pallas_call | solution.py:117
  240.9 2.8 %collective-permute-start.13 = (bf16[256,256]{0,1:T(8,128)(2,1)S(1)}, bf16[256,256]{0,1:T(8,128)(2,1)}, u32[]{:S(2)}, u32[]{:S(2)}) collective-permute-start(bf16[256,256]{0,1:T(8,128)(2,1)S(1)} %get-tuple-element.50), channel_id=1, source_target_pairs={{0,24},{8,0},{16,8},{24,16},{1,25},{9,1},{17,9},{25,17},{2,26},{10... | collective-permute-start | bytes 393224 | tf_op jit(solution)/shard_map/ppermute | solution.py:23
  247.0 3.2 %convolution_add_fusion.3 = f32[1024,256]{1,0:T(8,128)} fusion(f32[1024,256]{1,0:T(8,128)S(1)} %fusion.44, bf16[768,1024]{1,0:T(8,128)(2,1)} %bitcast.135, bf16[256,256]{0,1:T(8,128)(2,1)} %collective-permute-done.13, bf16[256,256]{0,1:T(8,128)(2,1)} %copy-done.19, bf16[256,256]{0,1:T(8,128)(2,1)} %copy-done.18), kind=kOutput, calls=%fused_computation.29 | convolution fusion | flops 404094976 | bytes 4063232 | tf_op jit(solution)/shard_map/dot_general | solution.py:18
  (194 shorter events, 45.1 us)
Async XLA Ops:
  7.2 74.3 %copy-start = (bf16[1,4096,256]{2,1,0:T(8,128)(2,1)S(1)}, bf16[1,4096,256]{2,1,0:T(8,128)(2,1)}, u32[]{:S(2)}) copy-start(bf16[1,4096,256]{2,1,0:T(8,128)(2,1)} %param.23) | copy-start | bytes 6291460
  7.2 156.7 %reduce-scatter.2.cloned.1.call-start = ((), (), s32[]{:S(2)}) async-start(), calls=%async_computation.1 | async-start | bytes 7077888 | tf_op jit(solution)/shard_map/reduce_scatter | solution.py:258
  97.8 14.8 %copy-start.11 = (bf16[256,128]{1,0:T(8,128)(2,1)S(1)}, bf16[256,128]{1,0:T(8,128)(2,1)}, u32[]{:S(2)}) copy-start(bf16[256,128]{1,0:T(8,128)(2,1)} %param.15) | copy-start | bytes 196612
  100.7 32.6 %collective-permute-start.8 = (bf16[260,128]{1,0:T(8,128)(2,1)S(1)}, bf16[260,128]{1,0:T(8,128)(2,1)S(1)}, u32[]{:S(2)}, u32[]{:S(2)}) collective-permute-start(bf16[260,128]{1,0:T(8,128)(2,1)S(1)} %pad_maximum_fusion.4), channel_id=1, source_target_pairs={{0,8},{8,16},{16,24},{24,0},{1,9},{9,17},{17,25},{25,1},{2,10},{10... | collective-permute-start | bytes 199688 | tf_op jit(solution)/shard_map/ppermute | solution.py:23
  107.1 26.3 %collective-permute-start.9 = (bf16[260,128]{1,0:T(8,128)(2,1)S(1)}, bf16[260,128]{1,0:T(8,128)(2,1)S(1)}, u32[]{:S(2)}, u32[]{:S(2)}) collective-permute-start(bf16[260,128]{1,0:T(8,128)(2,1)S(1)} %pad_maximum_fusion.4), channel_id=1, source_target_pairs={{0,16},{8,24},{16,0},{24,8},{1,17},{9,25},{17,1},{25,9},{2,18},{10... | collective-permute-start | bytes 199688 | tf_op jit(solution)/shard_map/ppermute | solution.py:23
  109.0 60.7 %collective-permute-start.10 = (bf16[260,128]{1,0:T(8,128)(2,1)S(1)}, bf16[260,128]{1,0:T(8,128)(2,1)}, u32[]{:S(2)}, u32[]{:S(2)}) collective-permute-start(bf16[260,128]{1,0:T(8,128)(2,1)S(1)} %pad_maximum_fusion.4), channel_id=1, source_target_pairs={{0,24},{8,0},{16,8},{24,16},{1,25},{9,1},{17,9},{25,17},{2,26},{10... | collective-permute-start | bytes 199688 | tf_op jit(solution)/shard_map/ppermute | solution.py:23
  109.5 22.7 %collective-permute-start.4 = (bf16[4,128]{1,0:T(4,128)(2,1)S(1)}, bf16[4,128]{1,0:T(4,128)(2,1)S(1)}, u32[]{:S(2)}, u32[]{:S(2)}) collective-permute-start(bf16[4,128]{1,0:T(4,128)(2,1)S(1)} %broadcast_in_dim.99), channel_id=1, source_target_pairs={{0,24},{8,0},{16,8},{24,16},{1,25},{9,1},{17,9},{25,17},{2,26},{10... | collective-permute-start | bytes 3080 | tf_op jit(solution)/shard_map/ppermute | solution.py:23
  111.5 20.8 %collective-permute-start.6 = (bf16[4,128]{1,0:T(4,128)(2,1)S(1)}, bf16[4,128]{1,0:T(4,128)(2,1)S(1)}, u32[]{:S(2)}, u32[]{:S(2)}) collective-permute-start(bf16[4,128]{1,0:T(4,128)(2,1)S(1)} %broadcast_in_dim.99), channel_id=1, source_target_pairs={{0,16},{8,24},{16,0},{24,8},{1,17},{9,25},{17,1},{25,9},{2,18},{10... | collective-permute-start | bytes 3080 | tf_op jit(solution)/shard_map/ppermute | solution.py:23
  112.5 8.4 %copy-start.30 = (f32[256]{0:T(256)}, f32[256]{0:T(256)S(1)}, u32[]{:S(2)}) copy-start(f32[256]{0:T(256)S(1)} %get-tuple-element.57) | copy-start | bytes 3076
  112.5 8.4 %copy-start.33 = (f32[256]{0:T(256)}, f32[256]{0:T(256)S(1)}, u32[]{:S(2)}) copy-start(f32[256]{0:T(256)S(1)} %get-tuple-element.55) | copy-start | bytes 3076
  112.5 8.4 %copy-start.35 = (f32[256]{0:T(256)}, f32[256]{0:T(256)S(1)}, u32[]{:S(2)}) copy-start(f32[256]{0:T(256)S(1)} %get-tuple-element.54) | copy-start | bytes 3076
  113.7 9.4 %slice-start.3 = ((s8[4718592]{0:T(1024)(128)(4,1)}), s8[4194304]{0:T(1024)(128)(4,1)S(1)}, s32[]{:S(2)}) async-start(s8[4718592]{0:T(1024)(128)(4,1)} %bitcast.157), calls=%async_computation.5 | async-start | bytes 8388608
  165.2 8.7 %collective-permute-start = (bf16[192,512]{1,0:T(8,128)(2,1)S(1)}, bf16[192,512]{1,0:T(8,128)(2,1)S(1)}, u32[]{:S(2)}, u32[]{:S(2)}) collective-permute-start(bf16[192,512]{1,0:T(8,128)(2,1)S(1)} %get-tuple-element.49), channel_id=1, source_target_pairs={{0,24},{8,0},{16,8},{24,16},{1,25},{9,1},{17,9},{25,17},{2,26},{10... | collective-permute-start | bytes 589832 | tf_op jit(solution)/shard_map/ppermute | solution.py:23
  168.6 16.7 %collective-permute-start.1 = (bf16[192,512]{1,0:T(8,128)(2,1)S(1)}, bf16[192,512]{1,0:T(8,128)(2,1)S(1)}, u32[]{:S(2)}, u32[]{:S(2)}) collective-permute-start(bf16[192,512]{1,0:T(8,128)(2,1)S(1)} %get-tuple-element.48), channel_id=1, source_target_pairs={{0,16},{8,24},{16,0},{24,8},{1,17},{9,25},{17,1},{25,9},{2,18},{10... | collective-permute-start | bytes 589832 | tf_op jit(solution)/shard_map/ppermute | solution.py:23
  168.6 16.7 %collective-permute-start.2 = (bf16[192,512]{1,0:T(8,128)(2,1)S(1)}, bf16[192,512]{1,0:T(8,128)(2,1)S(1)}, u32[]{:S(2)}, u32[]{:S(2)}) collective-permute-start(bf16[192,512]{1,0:T(8,128)(2,1)S(1)} %get-tuple-element.47), channel_id=1, source_target_pairs={{0,8},{8,16},{16,24},{24,0},{1,9},{9,17},{17,25},{25,1},{2,10},{10... | collective-permute-start | bytes 589832 | tf_op jit(solution)/shard_map/ppermute | solution.py:23
  185.3 17.3 %copy-start.8 = (bf16[4096,256]{1,0:T(8,128)(2,1)S(1)}, bf16[4096,256]{1,0:T(8,128)(2,1)}, u32[]{:S(2)}) copy-start(bf16[4096,256]{1,0:T(8,128)(2,1)} %param.18) | copy-start | bytes 6291460
  205.4 8.5 %copy-start.16 = (f32[256,256]{1,0:T(8,128)S(1)}, f32[256,256]{1,0:T(8,128)}, u32[]{:S(2)}) copy-start(f32[256,256]{1,0:T(8,128)} %copy-done.15) | copy-start | bytes 786436
  205.7 40.0 %collective-permute-start.11 = (bf16[256,256]{0,1:T(8,128)(2,1)S(1)}, bf16[256,256]{0,1:T(8,128)(2,1)S(1)}, u32[]{:S(2)}, u32[]{:S(2)}) collective-permute-start(bf16[256,256]{0,1:T(8,128)(2,1)S(1)} %get-tuple-element.50), channel_id=1, source_target_pairs={{0,8},{8,16},{16,24},{24,0},{1,9},{9,17},{17,25},{25,1},{2,10},{10... | collective-permute-start | bytes 393224 | tf_op jit(solution)/shard_map/ppermute | solution.py:23
  206.8 38.9 %collective-permute-start.12 = (bf16[256,256]{0,1:T(8,128)(2,1)S(1)}, bf16[256,256]{0,1:T(8,128)(2,1)S(1)}, u32[]{:S(2)}, u32[]{:S(2)}) collective-permute-start(bf16[256,256]{0,1:T(8,128)(2,1)S(1)} %get-tuple-element.50), channel_id=1, source_target_pairs={{0,16},{8,24},{16,0},{24,8},{1,17},{9,25},{17,1},{25,9},{2,18},{10... | collective-permute-start | bytes 393224 | tf_op jit(solution)/shard_map/ppermute | solution.py:23
  210.4 30.5 %collective-permute-start.3 = (bf16[256,128]{1,0:T(8,128)(2,1)S(1)}, bf16[256,128]{1,0:T(8,128)(2,1)S(1)}, u32[]{:S(2)}, u32[]{:S(2)}) collective-permute-start(bf16[256,128]{1,0:T(8,128)(2,1)S(1)} %convolution_convert_fusion.3), channel_id=1, source_target_pairs={{0,24},{8,0},{16,8},{24,16},{1,25},{9,1},{17,9},{25,17},{2,26},{10... | collective-permute-start | bytes 196616 | tf_op jit(solution)/shard_map/ppermute | solution.py:23
  213.3 30.4 %collective-permute-start.5 = (bf16[256,128]{1,0:T(8,128)(2,1)S(1)}, bf16[256,128]{1,0:T(8,128)(2,1)S(1)}, u32[]{:S(2)}, u32[]{:S(2)}) collective-permute-start(bf16[256,128]{1,0:T(8,128)(2,1)S(1)} %convolution_convert_fusion.3), channel_id=1, source_target_pairs={{0,16},{8,24},{16,0},{24,8},{1,17},{9,25},{17,1},{25,9},{2,18},{10... | collective-permute-start | bytes 196616 | tf_op jit(solution)/shard_map/ppermute | solution.py:23
  213.4 30.3 %collective-permute-start.7 = (bf16[256,128]{1,0:T(8,128)(2,1)S(1)}, bf16[256,128]{1,0:T(8,128)(2,1)S(1)}, u32[]{:S(2)}, u32[]{:S(2)}) collective-permute-start(bf16[256,128]{1,0:T(8,128)(2,1)S(1)} %convolution_convert_fusion.3), channel_id=1, source_target_pairs={{0,8},{8,16},{16,24},{24,0},{1,9},{9,17},{17,25},{25,1},{2,10},{10... | collective-permute-start | bytes 196616 | tf_op jit(solution)/shard_map/ppermute | solution.py:23
  216.3 27.4 %copy-start.27 = (f32[256]{0:T(256)S(1)}, f32[256]{0:T(256)}, u32[]{:S(2)}) copy-start(f32[256]{0:T(256)} %mul.197) | copy-start | bytes 3076
  240.9 6.1 %collective-permute-start.13 = (bf16[256,256]{0,1:T(8,128)(2,1)S(1)}, bf16[256,256]{0,1:T(8,128)(2,1)}, u32[]{:S(2)}, u32[]{:S(2)}) collective-permute-start(bf16[256,256]{0,1:T(8,128)(2,1)S(1)} %get-tuple-element.50), channel_id=1, source_target_pairs={{0,24},{8,0},{16,8},{24,16},{1,25},{9,1},{17,9},{25,17},{2,26},{10... | collective-permute-start | bytes 393224 | tf_op jit(solution)/shard_map/ppermute | solution.py:23
  (34 other events, 107.0 us)
Sparse Core Ops, SparseCore 0:
  97.9 65.9 reduce-scatter.1
where the time goes:
time: 258 us; the launch traced here: 257 us
  Pallas kernels  96.2 us (37%)
  matrix products  58.2 us (23%)
  waiting for transfers between devices  44.7 us (17%)
  starting transfers between devices  25.7 us (10%)
  between operations  14.9 us (6%)
  local copies, waits for them, and re-layouts  9.88 us (4%)
  other arithmetic  7.49 us (3%)
    pallas_call x3, Pallas kernels, spread(): pl.pallas_call(functools.partial(spread_kernel, n, count, far), out_shape...  96.2 us
    dot_general x44, matrix products, dot(): lax.dot_general(a, b, (((ca,), (cb,)), ((), ())), preferred_element_type=...  58.2 us
    reduce_scatter x1, waiting for transfers between devices, body(): summed = lax.psum_scatter(portion, 'tp', scatter_dimension=1, tiled=True)  30.1 us
    ppermute x14, starting transfers between devices, shift(): return lax.ppermute(x, 'sp', [(i, (i + by) % n) for i in range(n)])  25.7 us
    ppermute x14, waiting for transfers between devices, shift(): return lax.ppermute(x, 'sp', [(i, (i + by) % n) for i in range(n)])  14.6 us
    unnamed x90, local copies, waits for them, and re-layouts  5.62 us
  transfers between devices with their start and end apart: 15, of which 3 were waited for; matrix products, arithmetic and copies ran while one was open for 13% of the time, Pallas kernels for 8%

commit v1 on v0

--- a/solution.py
+++ b/solution.py
@@ -12,10 +12,474 @@
 
 F32 = jnp.float32
 BF16 = jnp.bfloat16
+MESH = pl.DeviceIdType.MESH
 
 
 def dot(a, b, ca=1, cb=0):
     return lax.dot_general(a, b, (((ca,), (cb,)), ((), ())), preferred_element_type=F32)
+
+
+class Links:
+    def __init__(self, send_sem, recv_sem):
+        self.send_sem, self.recv_sem = send_sem, recv_sem
+        self.used = 0
+        self.started = []
+
+    def slot(self):
+        self.used += 1
+        return self.used - 1
+
+    def copy(self, slot, src, dst, device):
+        return pltpu.make_async_remote_copy(
+            src_ref=src,
+            dst_ref=dst,
+            send_sem=self.send_sem.at[slot],
+            recv_sem=self.recv_sem.at[slot],
+            device_id=device,
+            device_id_type=MESH,
+        )
+
+    def start(self, slot, src, dst, device):
+        made = self.copy(slot, src, dst, device)
+        made.start()
+        self.started.append(made)
+
+    def arrived(self, slot, dst, device):
+        self.copy(slot, dst, dst, device).wait_recv()
+
+    def finish(self):
+        for made in self.started:
+            made.wait_send()
+
+
+class Spread:
+    def __init__(self, links, t, window):
+        self.links, self.window = links, window
+        self.other, self.across, self.along = ({"tp": t ^ bit} for bit in (1, 2, 4))
+        self.slots = [links.slot() for _ in range(9)]
+
+    def send(self, kind, bits, part, device):
+        w = self.window(bits, part)
+        self.links.start(self.slots[kind], w, w, device)
+
+    def got(self, kind, bits, part, device):
+        self.links.arrived(self.slots[kind], self.window(bits, part), device)
+
+    def p0(self):
+        self.send(1, 0, None, self.across)
+        self.send(2, 0, None, self.along)
+        self.send(5, 0, None, self.other)
+
+    def p1(self):
+        self.got(1, 2, None, self.across)
+        self.send(3, 2, 0, self.along)
+        self.send(6, 2, None, self.other)
+        self.got(2, 4, None, self.along)
+        self.send(4, 4, 1, self.across)
+        self.send(7, 4, None, self.other)
+
+    def p2(self):
+        self.got(3, 6, 0, self.along)
+        self.got(4, 6, 1, self.across)
+        self.send(8, 6, None, self.other)
+
+    def p3(self):
+        for kind, bits in ((5, 1), (6, 3), (7, 5), (8, 7)):
+            self.got(kind, bits, None, self.other)
+
+
+def greet(n, t, s):
+    peers = [{"tp": t ^ bit} for bit in (1, 2, 4)] + [{"sp": s ^ k} for k in range(1, n)]
+    barrier = pltpu.get_barrier_semaphore()
+    for peer in peers:
+        pl.semaphore_signal(barrier, inc=1, device_id=peer, device_id_type=MESH)
+    pl.semaphore_wait(barrier, len(peers))
+
+
+def main_kernel(
+    n,
+    ranks,
+    pieces,
+    onehot,
+    onehot_t,
+    row_weight,
+    mixed,
+    cotangent,
+    w_gate,
+    w_up,
+    w_down,
+    gw_out,
+    uw_out,
+    dw_out,
+    gm_out,
+    M,
+    C,
+    W2,
+    WD,
+    X,
+    S,
+    SX,
+    SS,
+    DGU,
+    HID,
+    HT,
+    PB,
+    RB,
+    SA,
+    RX,
+    RY,
+    BX,
+    BY,
+    RX2,
+    RY2,
+    FIN,
+    CB,
+    G,
+    GW,
+    UW,
+    DW,
+    send_sem,
+    recv_sem,
+    local_sem,
+):
+    t = lax.axis_index("tp")
+    s = lax.axis_index("sp")
+    tok, width = M.shape
+    hid = WD.shape[0]
+    cap = onehot.shape[0] // n
+    share = width // ranks
+    half_share = share // 2
+    blocks = PB.shape[0]
+    group = n // blocks
+    R = group * cap
+    strip = width // pieces
+    pw = strip // ranks
+    c = lax.rem(t, 2)
+    mx = lax.rem(t // 2, 2)
+    my = t // 4
+    links = Links(send_sem, recv_sem)
+    other, across, along = ({"tp": t ^ bit} for bit in (1, 2, 4))
+
+    def load(i, src, dst):
+        made = pltpu.make_async_copy(src, dst, local_sem.at[i])
+        made.start()
+        return made
+
+    loads = [
+        load(0, mixed, M),
+        load(1, cotangent, C),
+        load(2, w_gate, W2.at[:, pl.ds(0, hid)]),
+        load(3, w_up, W2.at[:, pl.ds(hid, hid)]),
+        load(4, w_down, WD),
+    ]
+    greet(n, t, s)
+    loads[0].wait()
+    loads[1].wait()
+
+    mine = pl.ds(pl.multiple_of(t * share, 128), share)
+    z_slots = [[links.slot() for _ in range(n)] for _ in range(2)]
+    m_part, c_part = M[:, mine], C[:, mine]
+    for k in range(1, n):
+        pick = onehot[pl.ds(k * cap, cap), :]
+        SX[k - 1] = dot(pick, m_part).astype(BF16)
+        SS[k - 1] = (dot(pick, c_part) * row_weight[pl.ds(k * cap, cap), :]).astype(BF16)
+        for a, (src, dst) in enumerate(((SX, X), (SS, S))):
+            links.start(
+                z_slots[a][k], src.at[k - 1], dst.at[pl.ds(k * cap, cap), mine], {"sp": s ^ k}
+            )
+
+    def local_rows(i, _):
+        at = pl.ds(pl.multiple_of(i * share, 128), share)
+        pick = onehot[pl.ds(0, cap), :]
+        X[pl.ds(0, cap), at] = dot(pick, M[:, at]).astype(BF16)
+        S[pl.ds(0, cap), at] = (dot(pick, C[:, at]) * row_weight[pl.ds(0, cap), :]).astype(BF16)
+        return 0
+
+    lax.fori_loop(0, ranks, local_rows, 0)
+
+    chunks = {}
+    for q in range(blocks):
+        first = cap if q == 0 else 0
+        if first == R:
+            continue
+        for a, ref in enumerate((X, S)):
+
+            def window(bits, part, ref=ref, row=q * R + first, count=R - first):
+                begin, size = (t ^ bits) * share, share
+                if part is not None:
+                    begin, size = begin + part * half_share, half_share
+                return ref.at[pl.ds(row, count), pl.ds(pl.multiple_of(begin, 128), size)]
+
+            chunks[(q, a)] = Spread(links, t, window)
+
+    def p0(q, a):
+        ref = (X, S)[a]
+        for k in range(q * group, (q + 1) * group):
+            if k:
+                links.arrived(z_slots[a][k], ref.at[pl.ds(k * cap, cap), mine], {"sp": s ^ k})
+        chunks[(q, a)].p0()
+
+    def p(stage, q, a):
+        getattr(chunks[(q, a)], stage)()
+
+    def expert(q):
+        r = pl.ds(q * R, R)
+        both = dot(X[r, :], W2[...])
+        gate, up = both[:, :hid], both[:, hid:]
+        sigma = jax.nn.sigmoid(gate)
+        act = gate * sigma
+        HID[r, :] = (act * up).astype(BF16)
+        d_act = dot(S[r, :], WD[...], 1, 1)
+        DGU[r, pl.ds(0, hid)] = (d_act * up * sigma * (1.0 + gate * (1.0 - sigma))).astype(BF16)
+        DGU[r, pl.ds(hid, hid)] = (d_act * act).astype(BF16)
+
+    def portion(q):
+        r = pl.ds(q * R, R)
+        step = 256
+        for j in range(pieces):
+
+            def some(i, _, j=j):
+                begin = pl.multiple_of(j * strip + i * step, 128)
+                tile = dot(DGU[r, :], W2[pl.ds(begin, step), :], 1, 1).astype(BF16)
+                if pw >= step:
+                    per = pw // step
+                    dest, off = i // per, lax.rem(i, per) * step
+                    at = pl.ds(pl.multiple_of(j * pw + off, 128), step)
+                    PB[q, lax.rem(dest, 2), dest // 2, :, at] = tile
+                else:
+                    at = pl.ds(j * pw, pw)
+                    PB[q, 0, i, :, at] = tile[:, :pw]
+                    PB[q, 1, i, :, at] = tile[:, pw:]
+                return 0
+
+            lax.fori_loop(0, strip // step, some, 0)
+
+    rs_slots = [[links.slot() for _ in range(5)] for _ in range(blocks)]
+    back_slots = [links.slot() for _ in range(n)]
+    lo, hi = pl.ds(0, half_share), pl.ds(half_share, half_share)
+
+    def r0(q):
+        links.start(rs_slots[q][0], PB.at[q, 1 - c], RB.at[q], other)
+
+    def r1(q):
+        links.arrived(rs_slots[q][0], RB.at[q], other)
+
+        def add(i, _):
+            SA[q, i // 2, lax.rem(i, 2)] = (PB[q, c, i].astype(F32) + RB[q, i].astype(F32)).astype(BF16)
+            return 0
+
+        lax.fori_loop(0, ranks // 2, add, 0)
+        links.start(rs_slots[q][1], SA.at[q, :, 1 - mx, :, lo], RX.at[q], across)
+        links.start(rs_slots[q][2], SA.at[q, 1 - my, :, :, hi], RY.at[q], along)
+
+    def r2(q):
+        links.arrived(rs_slots[q][1], RX.at[q], across)
+        for i in range(2):
+            BX[q, i] = (SA[q, i, mx, :, lo].astype(F32) + RX[q, i].astype(F32)).astype(BF16)
+        links.start(rs_slots[q][3], BX.at[q, 1 - my], RX2.at[q], along)
+        links.arrived(rs_slots[q][2], RY.at[q], along)
+        for i in range(2):
+            BY[q, i] = (SA[q, my, i, :, hi].astype(F32) + RY[q, i].astype(F32)).astype(BF16)
+        links.start(rs_slots[q][4], BY.at[q, 1 - mx], RY2.at[q], across)
+
+    def r3(q):
+        r = pl.ds(q * R, R)
+        links.arrived(rs_slots[q][3], RX2.at[q], along)
+        FIN[r, lo] = (BX[q, my].astype(F32) + RX2[q].astype(F32)).astype(BF16)
+        links.arrived(rs_slots[q][4], RY2.at[q], across)
+        FIN[r, hi] = (BY[q, mx].astype(F32) + RY2[q].astype(F32)).astype(BF16)
+        for k in range(q * group, (q + 1) * group):
+            rows = pl.ds(k * cap, cap)
+            if k:
+                links.start(back_slots[k], FIN.at[rows, :], CB.at[rows, :], {"sp": s ^ k})
+            else:
+                CB[rows, :] = FIN[rows, :]
+
+    def grads_gate_up(first, last):
+        def some(i, _):
+            at = pl.ds(pl.multiple_of(i * 256, 128), 256)
+            tile = dot(X[:, at], DGU[...], 0, 0).astype(BF16)
+            GW[at, :] = tile[:, :hid]
+            UW[at, :] = tile[:, hid:]
+            return 0
+
+        lax.fori_loop(first, last, some, 0)
+
+    def grads_down():
+        HT[...] = HID[...].T
+
+        def some(i, _):
+            at = pl.ds(pl.multiple_of(i * 512, 128), 512)
+            DW[:, at] = dot(HT[...], S[:, at]).astype(BF16)
+            return 0
+
+        lax.fori_loop(0, width // 512, some, 0)
+
+    order = [key for key in chunks]
+    count = len(order)
+
+    def forward(i):
+        if i < count:
+            p0(*order[i])
+        if 0 <= i - 1 < count:
+            p("p1", *order[i - 1])
+        if 0 <= i - 2 < count:
+            p("p2", *order[i - 2])
+
+    def whole(q):
+        for a in range(2):
+            if (q, a) in chunks:
+                p("p3", q, a)
+        expert(q)
+        portion(q)
+        r0(q)
+
+    for i in range(2, 5):
+        loads[i].wait()
+    if blocks == 4 and (0, 0) not in chunks:
+        forward(0)
+        expert(0)
+        forward(1)
+        portion(0)
+        r0(0)
+        forward(2)
+        r1(0)
+        forward(3)
+        r2(0)
+        forward(4)
+        whole(1)
+        r3(0)
+        forward(5)
+        r1(1)
+        forward(6)
+        whole(2)
+        r2(1)
+        forward(7)
+        r1(2)
+        r3(1)
+        whole(3)
+        r2(2)
+        r1(3)
+    else:
+        for i in range(count + 2):
+            forward(i)
+        for q in range(blocks):
+            whole(q)
+        for q in range(blocks):
+            r1(q)
+        for q in range(blocks - 1):
+            r2(q)
+        for q in range(blocks - 2):
+            r3(q)
+    tiles = width // 256
+    grads_gate_up(0, tiles // 4)
+    r3(blocks - 2)
+    r2(blocks - 1)
+    grads_gate_up(tiles // 4, tiles // 2)
+    r3(blocks - 1)
+    grads_gate_up(tiles // 2, tiles)
+    outs = [load(5, GW, gw_out), load(6, UW, uw_out)]
+    for k in range(1, n):
+        rows = pl.ds(k * cap, cap)
+        links.arrived(back_slots[k], CB.at[rows, :], {"sp": s ^ k})
+
+    half_tok = tok // 2
+    gathers = []
+    for i in range(2):
+
+        def window(bits, part, i=i):
+            row, rows = i * half_tok, half_tok
+            if part is not None:
+                row, rows = row + part * (half_tok // 2), half_tok // 2
+            return G.at[:, pl.ds(row, rows), pl.ds(pl.multiple_of((t ^ bits) * pw, 128), pw)]
+
+        gathers.append(Spread(links, t, window))
+    for i in range(2):
+        rows = pl.ds(i * half_tok, half_tok)
+        back = dot(onehot_t[rows, :], CB[...])
+        for j in range(pieces):
+            cot = C[rows, pl.ds(pl.multiple_of(j * strip + t * pw, 128), pw)].astype(F32)
+            G[j, rows, pl.ds(pl.multiple_of(t * pw, 128), pw)] = (
+                cot + back[:, j * pw : (j + 1) * pw]
+            ).astype(BF16)
+        gathers[i].p0()
+    grads_down()
+    outs.append(load(7, DW, dw_out))
+    for i in range(2):
+        gathers[i].p1()
+    for i in range(2):
+        gathers[i].p2()
+    for i in range(2):
+        gathers[i].p3()
+    for j in range(pieces):
+        outs.append(load(8 + j, G.at[j], gm_out.at[:, pl.ds(j * strip, strip)]))
+    links.finish()
+    for made in outs:
+        made.wait()
+
+
+def main_call(n, onehot, onehot_t, row_weight, mixed, cotangent, w_gate, w_up, w_down):
+    tok, width = mixed.shape
+    hid = w_gate.shape[1]
+    ranks = lax.axis_size("tp")
+    share = width // ranks
+    rows = onehot.shape[0]
+    cap = rows // n
+    pieces = n if (width // n // ranks) % 128 == 0 else 1
+    strip = width // pieces
+    blocks = 4 if n % 4 == 0 else n
+    R = rows // blocks
+    slots = 2 * n + 2 * blocks * 9 + 5 * blocks + n + 18
+    any_, vmem = pl.BlockSpec(memory_space=pl.ANY), pl.BlockSpec(memory_space=pltpu.VMEM)
+
+    def buf(*shape):
+        return pltpu.VMEM(shape, BF16)
+
+    return pl.pallas_call(
+        functools.partial(main_kernel, n, ranks, pieces),
+        out_shape=[
+            jax.ShapeDtypeStruct((width, hid), BF16),
+            jax.ShapeDtypeStruct((width, hid), BF16),
+            jax.ShapeDtypeStruct((hid, width), BF16),
+            jax.ShapeDtypeStruct((tok, width), BF16),
+        ],
+        in_specs=[vmem] * 3 + [any_] * 5,
+        out_specs=[any_] * 4,
+        scratch_shapes=[
+            buf(tok, width),
+            buf(tok, width),
+            buf(width, 2 * hid),
+            buf(hid, width),
+            buf(rows, width),
+            buf(rows, width),
+            buf(n - 1, cap, share),
+            buf(n - 1, cap, share),
+            buf(rows, 2 * hid),
+            buf(rows, hid),
+            buf(hid, rows),
+            buf(blocks, 2, ranks // 2, R, share),
+            buf(blocks, ranks // 2, R, share),
+            buf(blocks, 2, 2, R, share),
+            buf(blocks, 2, R, share // 2),
+            buf(blocks, 2, R, share // 2),
+            buf(blocks, 2, R, share // 2),
+            buf(blocks, 2, R, share // 2),
+            buf(blocks, R, share // 2),
+            buf(blocks, R, share // 2),
+            buf(rows, share),
+            buf(rows, share),
+            buf(pieces, tok, strip),
+            buf(width, hid),
+            buf(width, hid),
+            buf(hid, width),
+            pltpu.SemaphoreType.DMA((slots,)),
+            pltpu.SemaphoreType.DMA((slots,)),
+            pltpu.SemaphoreType.DMA((8 + pieces,)),
+        ],
+        compiler_params=pltpu.CompilerParams(
+            collective_id=1, has_side_effects=True, vmem_limit_bytes=60 * 1024 * 1024
+        ),
+    )(onehot, onehot_t, row_weight, mixed, cotangent, w_gate, w_up, w_down)
 
 
 def shift(x, by):
@@ -147,11 +611,9 @@
     tok, width = mixed.shape
     n = lax.axis_size("sp")
     cap = 3 * tok // n
-    share = width // lax.axis_size("tp")
     own = lax.axis_index("sp")
-    offset = lax.axis_index("tp") * share
-
-    rel = lax.rem(route_ids - own + n, n)
+
+    rel = jnp.bitwise_xor(route_ids, own)
     hit = rel[:, :, None] == jnp.arange(n, dtype=jnp.int32)[None, None, :]
     member = jnp.any(hit, axis=1)
     weight = jnp.sum(jnp.where(hit, route_weights[:, :, None], 0.0), axis=1)
@@ -161,18 +623,11 @@
     slot = jnp.where(member, slot, -1).T
     place = jnp.arange(cap, dtype=jnp.int32)
     chosen = slot[:, None, :] == place[None, :, None]
-    onehot = chosen.astype(BF16)
-    row_weight = jnp.sum(jnp.where(chosen, weight.T[:, None, :], 0.0), axis=2)
-
-    mixed_part = lax.dynamic_slice_in_dim(mixed, offset, share, 1)
-    cot_part = lax.dynamic_slice_in_dim(cotangent, offset, share, 1)
-    away = onehot[1:].reshape((n - 1) * cap, tok)
-    away_weight = row_weight[1:].reshape((n - 1) * cap, 1)
-    send_rows = dot(away, mixed_part).astype(BF16).reshape(n - 1, cap, share)
-    send_scaled = (dot(away, cot_part) * away_weight).astype(BF16).reshape(n - 1, cap, share)
-    rem_rows, rem_scaled = spread([send_rows, send_scaled], True, 1)
-    loc_rows = dot(onehot[0], mixed).astype(BF16)
-    loc_scaled = (dot(onehot[0], cotangent) * row_weight[0][:, None]).astype(BF16)
+    onehot = chosen.astype(BF16).reshape(n * cap, tok)
+    row_weight = jnp.sum(jnp.where(chosen, weight.T[:, None, :], 0.0), axis=2).reshape(n * cap, 1)
+    grad_gate, grad_up, grad_down, grad_mixed = main_call(
+        n, onehot, onehot.T, row_weight, mixed, cotangent, w_gate[0], w_up[0], w_down[0]
+    )
 
     heads = log_decay.shape[0]
     groups = write_keys.shape[1] // STATE
@@ -239,36 +694,6 @@
     )
     y = jnp.concatenate(outs, axis=1) + carried * leads_wide
     gated_b = (y * silu).astype(BF16)
-
-    def both(loc, rem, w, cb):
-        return jnp.concatenate([dot(loc, w, 1, cb), dot(rem, w, 1, cb)], axis=0)
-
-    def over_rows(loc, rem, d):
-        return (dot(loc, d[:cap], 0, 0) + dot(rem, d[cap:], 0, 0)).astype(BF16)
-
-    gate_pre = both(loc_rows, rem_rows, w_gate[0], 0)
-    up_pre = both(loc_rows, rem_rows, w_up[0], 0)
-    sigma = jax.nn.sigmoid(gate_pre)
-    act_gate = gate_pre * sigma
-    hidden = (act_gate * up_pre).astype(BF16)
-    d_hidden = both(loc_scaled, rem_scaled, w_down[0], 1)
-    d_gate = (d_hidden * up_pre * sigma * (1.0 + gate_pre * (1.0 - sigma))).astype(BF16)
-    d_up = (d_hidden * act_gate).astype(BF16)
-    portion = (dot(d_gate, w_gate[0], 1, 1) + dot(d_up, w_up[0], 1, 1)).astype(BF16)
-    summed = lax.psum_scatter(portion, "tp", scatter_dimension=1, tiled=True)
-    grad_gate = over_rows(loc_rows, rem_rows, d_gate)
-    grad_up = over_rows(loc_rows, rem_rows, d_up)
-    grad_down = (
-        dot(hidden[:cap], loc_scaled, 0, 0) + dot(hidden[cap:], rem_scaled, 0, 0)
-    ).astype(BF16)
-
-    came = [summed[:cap]] + [
-        shift(summed[j * cap : (j + 1) * cap], -j) for j in range(1, n)
-    ]
-    came = jnp.concatenate(came, axis=0)
-    back = dot(onehot.reshape(n * cap, tok), came, 0, 0)
-    grad_part = (cot_part.astype(F32) + back).astype(BF16)
-    (grad_mixed,) = spread([grad_part.reshape(2, tok // 2, share)], False, 2)
 
     out_grad = dot(grad_mixed, out_proj)
     quarter = width // n

time: 258 us -> 212 us (0.82)
  waiting for transfers between devices: 44.7 us -> 2.14 us
  Pallas kernels: 96.2 us -> 132 us
  matrix products: 58.2 us -> 28.9 us
  between operations: 14.9 us -> 1.07 us
  local copies, waits for them, and re-layouts: 9.88 us -> 18.8 us
  starting transfers between devices: 25.7 us -> 17.1 us
  other arithmetic: 7.49 us -> 11.2 us
    pallas_call x0 -> x1, Pallas kernels: none -> 111 us  [main_call(): pl.pallas_call(functools.partial(main_kernel, n, ranks, pieces), out_shap...]
    pallas_call x3 -> x1, Pallas kernels: 96.2 us -> 20.7 us  [spread(): pl.pallas_call(functools.partial(spread_kernel, n, count, far), out_shape...]
    reduce_scatter x1 -> x0, waiting for transfers between devices: 30.1 us -> none  [body(): summed = lax.psum_scatter(portion, 'tp', scatter_dimension=1, tiled=True)]
    dot_general x44 -> x25, matrix products: 58.2 us -> 28.9 us  [dot(): lax.dot_general(a, b, (((ca,), (cb,)), ((), ())), preferred_element_type=...]
    ppermute x14 -> x11, waiting for transfers between devices: 14.6 us -> 2.14 us  [shift(): return lax.ppermute(x, 'sp', [(i, (i + by) % n) for i in range(n)])]
    ppermute x14 -> x11, starting transfers between devices: 25.7 us -> 17.1 us  [shift(): return lax.ppermute(x, 'sp', [(i, (i + by) % n) for i in range(n)])]
    unnamed x90 -> x55, local copies, waits for them, and re-layouts: 5.62 us -> 11 us
  transfers between devices with their start and end apart: 15 -> 11, of which waited for: 3 -> 1; matrix products, arithmetic and copies ran while one was open for 13% -> 16% of each run, Pallas kernels for 8% -> 63%
where the time goes in v1:
time: 212 us; the launch traced here: 211 us
  Pallas kernels  132 us (62%)
  matrix products  28.9 us (14%)
  local copies, waits for them, and re-layouts  18.8 us (9%)
  starting transfers between devices  17.1 us (8%)
  other arithmetic  11.2 us (5%)
  waiting for transfers between devices  2.14 us (1%)
    pallas_call x1, Pallas kernels, main_call(): pl.pallas_call(functools.partial(main_kernel, n, ranks, pieces), out_shap...  111 us
    dot_general x25, matrix products, dot(): lax.dot_general(a, b, (((ca,), (cb,)), ((), ())), preferred_element_type=...  28.9 us
    pallas_call x1, Pallas kernels, spread(): pl.pallas_call(functools.partial(spread_kernel, n, count, far), out_shape...  20.7 us
    ppermute x11, starting transfers between devices, shift(): return lax.ppermute(x, 'sp', [(i, (i + by) % n) for i in range(n)])  17.1 us
    unnamed x55, local copies, waits for them, and re-layouts  11 us
  transfers between devices with their start and end apart: 11, of which 1 were waited for; matrix products, arithmetic and copies ran while one was open for 16% of the time, Pallas kernels for 63%

profile of v1, /device:TPU:0, one launch (start us, length us, event | category | flops | bytes accessed | tf_op | source)
XLA Modules:
  0.0 211.2 jit_solution(9869126996967780236)
XLA Ops:
  7.7 4.1 %collective-permute-start.6 = (bf16[260,128]{1,0:T(8,128)(2,1)}, bf16[260,128]{1,0:T(8,128)(2,1)}, u32[]{:S(2)}, u32[]{:S(2)}) collective-permute-start(bf16[260,128]{1,0:T(8,128)(2,1)} %pad_maximum_fusion.1), channel_id=1, source_target_pairs={{0,16},{8,24},{16,0},{24,8},{1,17},{9,25},{17,1},{25,9},{2,18},{10... | collective-permute-start | bytes 199688 | tf_op jit(solution)/shard_map/ppermute | solution.py:487
  11.8 1.6 collective-permute-start.5
  13.4 2.2 %collective-permute-start.7 = (bf16[260,128]{1,0:T(8,128)(2,1)}, bf16[260,128]{1,0:T(8,128)(2,1)}, u32[]{:S(2)}, u32[]{:S(2)}) collective-permute-start(bf16[260,128]{1,0:T(8,128)(2,1)} %pad_maximum_fusion.1), channel_id=1, source_target_pairs={{0,24},{8,0},{16,8},{24,16},{1,25},{9,1},{17,9},{25,17},{2,26},{10... | collective-permute-start | bytes 199688 | tf_op jit(solution)/shard_map/ppermute | solution.py:487
  18.7 1.4 copy.46
  25.7 1.8 fusion.30
  27.5 1.7 fusion.33
  31.0 111.3 %shard_map.188 = (bf16[4096,256]{1,0:T(8,128)(2,1)}, bf16[4096,256]{1,0:T(8,128)(2,1)}, bf16[256,4096]{1,0:T(8,128)(2,1)}, bf16[256,4096]{1,0:T(8,128)(2,1)}) custom-call(bf16[768,256]{1,0:T(8,128)(2,1)} %copy.47.onehot, bf16[256,768]{1,0:T(8,128)(2,1)} %fusion.86.onehot_t, f32[768,1]{1,0:T(8,128)} %reshape.101.row_weight, bf16[256,4096]{1,0:T(8,128)(2,1)} %mixed.1, ...), custom_call_target="tpu_custom_call" | custom-call | tf_op jit(solution)/shard_map/pallas_call | solution.py:438
  142.4 2.6 %fusion.62 = f32[256,256]{0,1:T(8,128)S(1)} fusion(bf16[256,4096]{1,0:T(8,128)(2,1)} %get-tuple-element.12, bf16[4096,256]{1,0:T(8,128)(2,1)S(1)} %copy-done), kind=kOutput, calls=%fused_computation.120 | convolution fusion | flops 536870912 | bytes 4456448 | tf_op jit(solution)/shard_map/dot_general | solution.py:19
  146.8 20.7 %shard_map.189 = bf16[3,256,1024]{2,1,0:T(8,128)(2,1)} custom-call(bf16[3,256,128]{2,1,0:T(8,128)(2,1)} %pad_maximum_fusion.refs_0_), custom_call_target="tpu_custom_call" | custom-call | tf_op jit(solution)/shard_map/pallas_call | solution.py:581
  172.0 1.9 multiply_convert_fusion
  173.8 1.8 fusion.43
  175.6 1.8 fusion.46
  177.5 1.8 fusion.49
  180.1 3.7 %collective-permute-start.2 = (bf16[256,128]{1,0:T(8,128)(2,1)}, bf16[256,128]{1,0:T(8,128)(2,1)}, u32[]{:S(2)}, u32[]{:S(2)}) collective-permute-start(bf16[256,128]{1,0:T(8,128)(2,1)} %convolution_convert_fusion.1), channel_id=1, source_target_pairs={{0,16},{8,24},{16,0},{24,8},{1,17},{9,25},{17,1},{25,9},{2,18},{10... | collective-permute-start | bytes 196616 | tf_op jit(solution)/shard_map/ppermute | solution.py:487
  186.0 1.4 collective-permute-start.10
  187.3 2.0 collective-permute-start.9
  190.2 1.4 fusion.12
  191.9 1.7 copy.53
  194.3 1.9 fusion.8
  196.2 1.7 copy.52
  197.9 2.0 fusion.9
  199.8 2.1 %collective-permute-done.9 = bf16[256,256]{0,1:T(8,128)(2,1)} collective-permute-done((bf16[256,256]{0,1:T(8,128)(2,1)S(1)}, bf16[256,256]{0,1:T(8,128)(2,1)}, u32[]{:S(2)}, u32[]{:S(2)}) %collective-permute-start.9) | collective-permute-done | bytes 131104 | tf_op jit(solution)/shard_map/ppermute | solution.py:487
  201.9 3.2 %convolution_add_fusion = f32[1024,256]{1,0:T(8,128)} fusion(f32[1024,256]{1,0:T(8,128)S(1)} %fusion.12, bf16[768,1024]{1,0:T(8,128)(2,1)} %bitcast.86, bf16[256,256]{0,1:T(8,128)(2,1)} %collective-permute-done.10, bf16[256,256]{0,1:T(8,128)(2,1)} %collective-permute-done.9, bf16[256,256]{0,1:T(8,128)(2,1)} %collective-permute-done.8), kind=kOutput, calls=%fused_computation | convolution fusion | flops 404094976 | bytes 4063232 | tf_op jit(solution)/shard_map/dot_general | solution.py:19
  205.2 1.3 copy.65
  (125 shorter events, 33.1 us)
Async XLA Ops:
  0.6 141.8 %copy-start = (bf16[4096,256]{1,0:T(8,128)(2,1)S(1)}, bf16[4096,256]{1,0:T(8,128)(2,1)}, u32[]{:S(2)}) copy-start(bf16[4096,256]{1,0:T(8,128)(2,1)} %param.18) | copy-start | bytes 6291460
  7.7 160.9 %collective-permute-start.6 = (bf16[260,128]{1,0:T(8,128)(2,1)}, bf16[260,128]{1,0:T(8,128)(2,1)}, u32[]{:S(2)}, u32[]{:S(2)}) collective-permute-start(bf16[260,128]{1,0:T(8,128)(2,1)} %pad_maximum_fusion.1), channel_id=1, source_target_pairs={{0,16},{8,24},{16,0},{24,8},{1,17},{9,25},{17,1},{25,9},{2,18},{10... | collective-permute-start | bytes 199688 | tf_op jit(solution)/shard_map/ppermute | solution.py:487
  11.8 157.8 %collective-permute-start.5 = (bf16[260,128]{1,0:T(8,128)(2,1)}, bf16[260,128]{1,0:T(8,128)(2,1)}, u32[]{:S(2)}, u32[]{:S(2)}) collective-permute-start(bf16[260,128]{1,0:T(8,128)(2,1)} %pad_maximum_fusion.1), channel_id=1, source_target_pairs={{0,8},{8,16},{16,24},{24,0},{1,9},{9,17},{17,25},{25,1},{2,10},{10... | collective-permute-start | bytes 199688 | tf_op jit(solution)/shard_map/ppermute | solution.py:487
  13.4 157.6 %collective-permute-start.7 = (bf16[260,128]{1,0:T(8,128)(2,1)}, bf16[260,128]{1,0:T(8,128)(2,1)}, u32[]{:S(2)}, u32[]{:S(2)}) collective-permute-start(bf16[260,128]{1,0:T(8,128)(2,1)} %pad_maximum_fusion.1), channel_id=1, source_target_pairs={{0,24},{8,0},{16,8},{24,16},{1,25},{9,1},{17,9},{25,17},{2,26},{10... | collective-permute-start | bytes 199688 | tf_op jit(solution)/shard_map/ppermute | solution.py:487
  15.6 151.9 %collective-permute-start.1 = (bf16[4,128]{1,0:T(4,128)(2,1)}, bf16[4,128]{1,0:T(4,128)(2,1)}, u32[]{:S(2)}, u32[]{:S(2)}) collective-permute-start(bf16[4,128]{1,0:T(4,128)(2,1)} %broadcast_in_dim.99), channel_id=1, source_target_pairs={{0,24},{8,0},{16,8},{24,16},{1,25},{9,1},{17,9},{25,17},{2,26},{10... | collective-permute-start | bytes 3080 | tf_op jit(solution)/shard_map/ppermute | solution.py:487
  15.6 151.9 %collective-permute-start.3 = (bf16[4,128]{1,0:T(4,128)(2,1)}, bf16[4,128]{1,0:T(4,128)(2,1)}, u32[]{:S(2)}, u32[]{:S(2)}) collective-permute-start(bf16[4,128]{1,0:T(4,128)(2,1)} %broadcast_in_dim.99), channel_id=1, source_target_pairs={{0,16},{8,24},{16,0},{24,8},{1,17},{9,25},{17,1},{25,9},{2,18},{10... | collective-permute-start | bytes 3080 | tf_op jit(solution)/shard_map/ppermute | solution.py:487
  21.1 8.2 %copy-start.6 = (bf16[256,256]{1,0:T(8,128)(2,1)S(1)}, bf16[256,256]{1,0:T(8,128)(2,1)}, u32[]{:S(2)}) copy-start(bf16[256,256]{1,0:T(8,128)(2,1)} %param.13) | copy-start | bytes 393220
  25.6 116.7 %copy-start.8 = (f32[256,256]{1,0:T(8,128)}, f32[256,256]{1,0:T(8,128)S(1)}, u32[]{:S(2)}) copy-start(f32[256,256]{1,0:T(8,128)S(1)} %fusion.61) | copy-start | bytes 786436
  25.7 116.7 %copy-start.14 = (f32[256]{0:T(256)}, f32[256]{0:T(256)S(1)}, u32[]{:S(2)}) copy-start(f32[256]{0:T(256)S(1)} %get-tuple-element.53) | copy-start | bytes 3076
  25.7 116.7 %copy-start.16 = (f32[256]{0:T(256)}, f32[256]{0:T(256)S(1)}, u32[]{:S(2)}) copy-start(f32[256]{0:T(256)S(1)} %get-tuple-element.54) | copy-start | bytes 3076
  25.7 116.7 %copy-start.18 = (f32[256]{0:T(256)}, f32[256]{0:T(256)S(1)}, u32[]{:S(2)}) copy-start(f32[256]{0:T(256)S(1)} %get-tuple-element.51) | copy-start | bytes 3076
  25.7 116.7 %copy-start.21 = (f32[256]{0:T(256)}, f32[256]{0:T(256)S(1)}, u32[]{:S(2)}) copy-start(f32[256]{0:T(256)S(1)} %get-tuple-element.52) | copy-start | bytes 3076
  146.7 27.1 %copy-start.22 = (f32[256]{0:T(256)S(1)}, f32[256]{0:T(256)}, u32[]{:S(2)}) copy-start(f32[256]{0:T(256)} %copy-done.21) | copy-start | bytes 3076
  146.7 28.9 %copy-start.15 = (f32[256]{0:T(256)S(1)}, f32[256]{0:T(256)}, u32[]{:S(2)}) copy-start(f32[256]{0:T(256)} %copy-done.14) | copy-start | bytes 3076
  167.5 10.0 %copy-start.17 = (f32[256]{0:T(256)S(1)}, f32[256]{0:T(256)}, u32[]{:S(2)}) copy-start(f32[256]{0:T(256)} %copy-done.16) | copy-start | bytes 3076
  168.6 15.3 %copy-start.7 = (bf16[256,256]{1,0:T(8,128)(2,1)S(1)}, bf16[256,256]{1,0:T(8,128)(2,1)}, u32[]{:S(2)}) copy-start(bf16[256,256]{1,0:T(8,128)(2,1)} %param.13) | copy-start | bytes 393220
  168.6 15.3 %copy-start.19 = (f32[256]{0:T(256)S(1)}, f32[256]{0:T(256)}, u32[]{:S(2)}) copy-start(f32[256]{0:T(256)} %copy-done.18) | copy-start | bytes 3076
  180.1 13.5 %collective-permute-start.4 = (bf16[256,128]{1,0:T(8,128)(2,1)}, bf16[256,128]{1,0:T(8,128)(2,1)}, u32[]{:S(2)}, u32[]{:S(2)}) collective-permute-start(bf16[256,128]{1,0:T(8,128)(2,1)} %convolution_convert_fusion.1), channel_id=1, source_target_pairs={{0,8},{8,16},{16,24},{24,0},{1,9},{9,17},{17,25},{25,1},{2,10},{10... | collective-permute-start | bytes 196616 | tf_op jit(solution)/shard_map/ppermute | solution.py:487
  180.1 14.2 %collective-permute-start.2 = (bf16[256,128]{1,0:T(8,128)(2,1)}, bf16[256,128]{1,0:T(8,128)(2,1)}, u32[]{:S(2)}, u32[]{:S(2)}) collective-permute-start(bf16[256,128]{1,0:T(8,128)(2,1)} %convolution_convert_fusion.1), channel_id=1, source_target_pairs={{0,16},{8,24},{16,0},{24,8},{1,17},{9,25},{17,1},{25,9},{2,18},{10... | collective-permute-start | bytes 196616 | tf_op jit(solution)/shard_map/ppermute | solution.py:487
  183.8 10.5 %collective-permute-start = (bf16[256,128]{1,0:T(8,128)(2,1)}, bf16[256,128]{1,0:T(8,128)(2,1)}, u32[]{:S(2)}, u32[]{:S(2)}) collective-permute-start(bf16[256,128]{1,0:T(8,128)(2,1)} %convolution_convert_fusion.1), channel_id=1, source_target_pairs={{0,24},{8,0},{16,8},{24,16},{1,25},{9,1},{17,9},{25,17},{2,26},{10... | collective-permute-start | bytes 196616 | tf_op jit(solution)/shard_map/ppermute | solution.py:487
  184.4 7.2 %copy-start.9 = (f32[256,256]{1,0:T(8,128)S(1)}, f32[256,256]{1,0:T(8,128)}, u32[]{:S(2)}) copy-start(f32[256,256]{1,0:T(8,128)} %copy-done.8) | copy-start | bytes 786436
  186.0 13.9 %collective-permute-start.10 = (bf16[256,256]{0,1:T(8,128)(2,1)S(1)}, bf16[256,256]{0,1:T(8,128)(2,1)}, u32[]{:S(2)}, u32[]{:S(2)}) collective-permute-start(bf16[256,256]{0,1:T(8,128)(2,1)S(1)} %get-tuple-element.47), channel_id=1, source_target_pairs={{0,24},{8,0},{16,8},{24,16},{1,25},{9,1},{17,9},{25,17},{2,26},{10... | collective-permute-start | bytes 393224 | tf_op jit(solution)/shard_map/ppermute | solution.py:487
  187.3 14.6 %collective-permute-start.9 = (bf16[256,256]{0,1:T(8,128)(2,1)S(1)}, bf16[256,256]{0,1:T(8,128)(2,1)}, u32[]{:S(2)}, u32[]{:S(2)}) collective-permute-start(bf16[256,256]{0,1:T(8,128)(2,1)S(1)} %get-tuple-element.47), channel_id=1, source_target_pairs={{0,16},{8,24},{16,0},{24,8},{1,17},{9,25},{17,1},{25,9},{2,18},{10... | collective-permute-start | bytes 393224 | tf_op jit(solution)/shard_map/ppermute | solution.py:487
  193.6 8.4 %collective-permute-start.8 = (bf16[256,256]{0,1:T(8,128)(2,1)S(1)}, bf16[256,256]{0,1:T(8,128)(2,1)}, u32[]{:S(2)}, u32[]{:S(2)}) collective-permute-start(bf16[256,256]{0,1:T(8,128)(2,1)S(1)} %get-tuple-element.47), channel_id=1, source_target_pairs={{0,8},{8,16},{16,24},{24,0},{1,9},{9,17},{17,25},{25,1},{2,10},{10... | collective-permute-start | bytes 393224 | tf_op jit(solution)/shard_map/ppermute | solution.py:487
  (10 other events, 32.8 us)

commit v2 on v1

v2 whole, which is shorter than its diff:
```python
import functools

import jax
import jax.numpy as jnp
from jax import lax
from jax.experimental import pallas as pl
from jax.experimental.pallas import tpu as pltpu
from jax.sharding import PartitionSpec as P

HEAD_DIM = 64
STATE = 128

F32 = jnp.float32
BF16 = jnp.bfloat16
MESH = pl.DeviceIdType.MESH


def dot(a, b, ca=1, cb=0):
    return lax.dot_general(a, b, (((ca,), (cb,)), ((), ())), preferred_element_type=F32)


class Links:
    def __init__(self, send_sem, recv_sem):
        self.send_sem, self.recv_sem = send_sem, recv_sem
        self.used = 0
        self.started = []

    def slot(self):
        self.used += 1
        return self.used - 1

    def copy(self, slot, src, dst, device):
        return pltpu.make_async_remote_copy(
            src_ref=src,
            dst_ref=dst,
            send_sem=self.send_sem.at[slot],
            recv_sem=self.recv_sem.at[slot],
            device_id=device,
            device_id_type=MESH,
        )

    def start(self, slot, src, dst, device):
        made = self.copy(slot, src, dst, device)
        made.start()
        self.started.append(made)

    def arrived(self, slot, dst, device):
        self.copy(slot, dst, dst, device).wait_recv()

    def finish(self):
        for made in self.started:
            made.wait_send()


class Spread:
    def __init__(self, links, t, window):
        self.links, self.window = links, window
        self.other, self.across, self.along = ({"tp": t ^ bit} for bit in (1, 2, 4))
        self.slots = [links.slot() for _ in range(9)]

    def send(self, kind, bits, part, device):
        w = self.window(bits, part)
        self.links.start(self.slots[kind], w, w, device)

    def got(self, kind, bits, part, device):
        self.links.arrived(self.slots[kind], self.window(bits, part), device)

    def p0(self):
        self.send(1, 0, None, self.across)
        self.send(2, 0, None, self.along)
        self.send(5, 0, None, self.other)

    def p1(self):
        self.got(1, 2, None, self.across)
        self.send(3, 2, 0, self.along)
        self.send(6, 2, None, self.other)
        self.got(2, 4, None, self.along)
        self.send(4, 4, 1, self.across)
        self.send(7, 4, None, self.other)

    def p2(self):
        self.got(3, 6, 0, self.along)
        self.got(4, 6, 1, self.across)
        self.send(8, 6, None, self.other)

    def p3(self):
        for kind, bits in ((5, 1), (6, 3), (7, 5), (8, 7)):
            self.got(kind, bits, None, self.other)


def greet(n, t, s):
    peers = [{"tp": t ^ bit} for bit in (1, 2, 4)] + [{"sp": s ^ k} for k in range(1, n)]
    barrier = pltpu.get_barrier_semaphore()
    for peer in peers:
        pl.semaphore_signal(barrier, inc=1, device_id=peer, device_id_type=MESH)
    pl.semaphore_wait(barrier, len(peers))


def main_kernel(
    n,
    ranks,
    pieces,
    ids_in,
    weights_in,
    mixed,
    cotangent,
    w_gate,
    w_up,
    w_down,
    values_in,
    writes_in,
    reads_in,
    decay_in,
    gate_in,
    proj_in,
    value_out,
    write_out,
    read_out,
    gate_out,
    *refs,
):
    outs_proj = refs[: 1 if pieces == n else 2]
    gw_out, uw_out, dw_out = refs[len(outs_proj) : len(outs_proj) + 3]
    (
        IDS, RW, M, C, W2, WD, X, S, SX, SS, ONE, WCOL, DGU, HID, HT,
        PB, RB, RX, RY, RX2, RY2, FIN, CB, G, GW, UW, DW,
        TV, WK, RK, LD, OGT, OP, LW, TW, Y, DEC, KT, TLD, END, TOT, BK, ENT, GB, F,
        OG, OB, LED, DWF, DV, DWK, DRK, DGT, PJ,
        send_sem, recv_sem, local_sem,
    ) = refs[len(outs_proj) + 3 :]
    t = lax.axis_index("tp")
    s = lax.axis_index("sp")
    tok, width = M.shape
    hid = WD.shape[0]
    cap = CB.shape[0] // n
    share = width // ranks
    half_share = share // 2
    blocks = PB.shape[0]
    group = n // blocks
    R = group * cap
    strip = width // pieces
    pw = strip // ranks
    heads = LD.shape[0]
    groups = WK.shape[1] // STATE
    per_group = heads // groups
    chan = per_group * HEAD_DIM
    c = lax.rem(t, 2)
    mx = lax.rem(t // 2, 2)
    my = t // 4
    links = Links(send_sem, recv_sem)
    other, across, along = ({"tp": t ^ bit} for bit in (1, 2, 4))
    loaded = [0]

    def load(src, dst):
        made = pltpu.make_async_copy(src, dst, local_sem.at[loaded[0]])
        loaded[0] += 1
        made.start()
        return made

    first_loads = [load(ids_in, IDS), load(weights_in, RW), load(mixed, M), load(cotangent, C)]
    mix_loads = [
        load(decay_in, LD),
        load(writes_in, WK),
        load(values_in, TV),
        load(reads_in, RK),
        load(gate_in, OGT),
    ]
    expert_loads = [
        load(w_gate, W2.at[:, pl.ds(0, hid)]),
        load(w_up, W2.at[:, pl.ds(hid, hid)]),
        load(w_down, WD),
    ]
    proj_load = load(proj_in, OP)
    greet(n, t, s)
    for made in first_loads:
        made.wait()

    rows_n = max(n, 8)
    lane = lax.broadcasted_iota(jnp.int32, (rows_n, tok), 0) ^ s
    names = [IDS[i : i + 1, :] == lane for i in range(IDS.shape[0])]
    member = functools.reduce(jnp.logical_or, names)
    weight = sum(jnp.where(names[i], RW[i : i + 1, :], 0.0) for i in range(IDS.shape[0]))
    row_of = lax.broadcasted_iota(jnp.int32, (tok, tok), 0)
    col_of = lax.broadcasted_iota(jnp.int32, (tok, tok), 1)
    earlier = (row_of < col_of).astype(F32).astype(BF16)
    slot = dot(member.astype(F32).astype(BF16), earlier)
    slot = jnp.where(member, slot, -1.0).astype(jnp.int32)
    place = lax.broadcasted_iota(jnp.int32, (cap, tok), 0)

    mine = pl.ds(pl.multiple_of(t * share, 128), share)
    z_slots = [[links.slot() for _ in range(n)] for _ in range(2)]
    m_part, c_part = M[:, mine], C[:, mine]
    for k in list(range(1, n)) + [0]:
        rows = pl.ds(k * cap, cap)
        chosen = slot[k : k + 1, :] == place
        pick = chosen.astype(F32).astype(BF16)
        row_weight = jnp.sum(jnp.where(chosen, weight[k : k + 1, :], 0.0), axis=1, keepdims=True)
        ONE[rows, :] = pick
        if k:
            SX[k - 1] = dot(pick, m_part).astype(BF16)
            SS[k - 1] = (dot(pick, c_part) * row_weight).astype(BF16)
            for a, (src, dst) in enumerate(((SX, X), (SS, S))):
                links.start(z_slots[a][k], src.at[k - 1], dst.at[rows, mine], {"sp": s ^ k})
        else:
            WCOL[...] = jnp.broadcast_to(row_weight, WCOL.shape)

    def local_rows():
        def some(i, _):
            at = pl.ds(pl.multiple_of(i * share, 128), share)
            pick = ONE[pl.ds(0, cap), :]
            X[pl.ds(0, cap), at] = dot(pick, M[:, at]).astype(BF16)
            S[pl.ds(0, cap), at] = (dot(pick, C[:, at]) * WCOL[:, :1]).astype(BF16)
            return 0

        lax.fori_loop(0, ranks, some, 0)

    chunks = {}
    for q in range(blocks):
        first = cap if q == 0 else 0
        if first == R:
            continue
        for a, ref in enumerate((X, S)):

            def window(bits, part, ref=ref, row=q * R + first, count=R - first):
                begin, size = (t ^ bits) * share, share
                if part is not None:
                    begin, size = begin + part * half_share, half_share
                return ref.at[pl.ds(row, count), pl.ds(pl.multiple_of(begin, 128), size)]

            chunks[(q, a)] = Spread(links, t, window)

    def p0(q, a):
        ref = (X, S)[a]
        for k in range(q * group, (q + 1) * group):
            if k:
                links.arrived(z_slots[a][k], ref.at[pl.ds(k * cap, cap), mine], {"sp": s ^ k})
        chunks[(q, a)].p0()

    def expert(q):
        r = pl.ds(q * R, R)
        both = dot(X[r, :], W2[...])
        gate, up = both[:, :hid], both[:, hid:]
        sigma = jax.nn.sigmoid(gate)
        act = gate * sigma
        HID[r, :] = (act * up).astype(BF16)
        d_act = dot(S[r, :], WD[...], 1, 1)
        DGU[r, pl.ds(0, hid)] = (d_act * up * sigma * (1.0 + gate * (1.0 - sigma))).astype(BF16)
        DGU[r, pl.ds(hid, hid)] = (d_act * act).astype(BF16)

    def portion(q):
        r = pl.ds(q * R, R)
        step = 256
        for j in range(pieces):

            def some(i, _, j=j):
                begin = pl.multiple_of(j * strip + i * step, 128)
                tile = dot(DGU[r, :], W2[pl.ds(begin, step), :], 1, 1).astype(BF16)
                if pw >= step:
                    per = pw // step
                    dest, off = i // per, lax.rem(i, per) * step
                    at = pl.ds(pl.multiple_of(j * pw + off, 128), step)
                    PB[q, lax.rem(dest, 2), dest // 4, lax.rem(dest // 2, 2), :, at] = tile
                else:
                    at = pl.ds(j * pw, pw)
                    PB[q, 0, i // 2, lax.rem(i, 2), :, at] = tile[:, :pw]
                    PB[q, 1, i // 2, lax.rem(i, 2), :, at] = tile[:, pw:]
                return 0

            lax.fori_loop(0, strip // step, some, 0)

    rs_slots = [[links.slot() for _ in range(5)] for _ in range(blocks)]
    back_slots = [links.slot() for _ in range(n)]
    lo, hi = pl.ds(0, half_share), pl.ds(half_share, half_share)

    def r0(q):
        links.start(rs_slots[q][0], PB.at[q, 1 - c], RB.at[q], other)

    def r1(q):
        links.arrived(rs_slots[q][0], RB.at[q], other)

        def add(i, _):
            a, b = i // 2, lax.rem(i, 2)
            RB[q, a, b] = (PB[q, c, a, b].astype(F32) + RB[q, a, b].astype(F32)).astype(BF16)
            return 0

        lax.fori_loop(0, ranks // 2, add, 0)
        links.start(rs_slots[q][1], RB.at[q, :, 1 - mx, :, lo], RX.at[q], across)
        links.start(rs_slots[q][2], RB.at[q, 1 - my, :, :, hi], RY.at[q], along)

    def r2(q):
        links.arrived(rs_slots[q][1], RX.at[q], across)
        for i in range(2):
            RX[q, i] = (RB[q, i, mx, :, lo].astype(F32) + RX[q, i].astype(F32)).astype(BF16)
        links.start(rs_slots[q][3], RX.at[q, 1 - my], RX2.at[q], along)
        links.arrived(rs_slots[q][2], RY.at[q], along)
        for i in range(2):
            RY[q, i] = (RB[q, my, i, :, hi].astype(F32) + RY[q, i].astype(F32)).astype(BF16)
        links.start(rs_slots[q][4], RY.at[q, 1 - mx], RY2.at[q], across)

    def r3(q):
        r = pl.ds(q * R, R)
        links.arrived(rs_slots[q][3], RX2.at[q], along)
        FIN[r, lo] = (RX[q, my].astype(F32) + RX2[q].astype(F32)).astype(BF16)
        links.arrived(rs_slots[q][4], RY2.at[q], across)
        FIN[r, hi] = (RY[q, mx].astype(F32) + RY2[q].astype(F32)).astype(BF16)
        for k in range(q * group, (q + 1) * group):
            rows = pl.ds(k * cap, cap)
            if k:
                links.start(back_slots[k], FIN.at[rows, :], CB.at[rows, :], {"sp": s ^ k})
            else:
                CB[rows, :] = FIN[rows, :]

    def grads_gate_up(first, last):
        def some(i, _):
            at = pl.ds(pl.multiple_of(i * 256, 128), 256)
            tile = dot(X[:, at], DGU[...], 0, 0).astype(BF16)
            GW[at, :] = tile[:, :hid]
            UW[at, :] = tile[:, hid:]
            return 0

        lax.fori_loop(first, last, some, 0)

    def grads_down():
        HT[...] = HID[...].T

        def some(i, _):
            at = pl.ds(pl.multiple_of(i * 512, 128), 512)
            DW[:, at] = dot(HT[...], S[:, at]).astype(BF16)
            return 0

        lax.fori_loop(0, width // 512, some, 0)

    head_of = lax.broadcasted_iota(jnp.int32, (tok, chan), 1) // HEAD_DIM
    end_slots = [[links.slot() for _ in range(n)] for _ in range(2)]
    gated_slots = [links.slot() for _ in range(n)]
    state_slots = [links.slot() for _ in range(n)]

    def keys(ref, g):
        return ref[:, g * STATE : (g + 1) * STATE]

    def wide(columns):
        return jnp.concatenate(
            [jnp.broadcast_to(columns[:, h : h + 1], (tok, HEAD_DIM)) for h in range(heads)], axis=1
        )

    def everyone(slots, src, dst):
        for k in range(1, n):
            links.start(slots[k], src, dst(k), {"sp": s ^ k})

    def mixer_ends():
        for made in mix_loads:
            made.wait()
        pad = max(heads, 8) - heads
        decays = LD[...]
        if pad:
            decays = jnp.concatenate([decays, jnp.zeros((pad, tok), F32)], axis=0)
        upto = (row_of <= col_of).astype(F32)
        cumul = lax.dot_general(
            decays,
            upto,
            (((1,), (0,)), ((), ())),
            precision=lax.Precision.HIGHEST,
            preferred_element_type=F32,
        )
        total = cumul[:, tok - 1 :]
        TOT[s] = jnp.broadcast_to(total, TOT.shape[1:])
        columns = cumul.T
        spread = wide(columns)
        LW[...] = jnp.exp(spread)
        tails = jnp.exp(spread[tok - 1 :, :] - spread)
        TW[...] = tails
        TLD[...] = (TV[...].astype(F32) * tails).astype(BF16)
        for g in range(groups):
            at = pl.ds(g * chan, chan)
            END[s, at, :] = dot(TLD[:, at], keys(WK, g), 0, 0).astype(BF16)
        everyone(end_slots[0], END.at[s], lambda k: END.at[s])
        everyone(end_slots[1], TOT.at[s], lambda k: TOT.at[s])
        for h in range(heads):
            span = columns[:, h : h + 1] - cumul[h : h + 1, :]
            DEC[h] = jnp.exp(jnp.where(row_of >= col_of, span, -jnp.inf))

    def mixer_inner():
        for g in range(groups):
            scores = dot(keys(RK, g), keys(WK, g), 1, 1)
            at = pl.ds(g * chan, chan)
            inner = jnp.zeros((tok, chan), F32)
            for r in range(per_group):
                h = g * per_group + r
                kept = scores * DEC[h]
                KT[h] = kept.T.astype(BF16)
                inner = jnp.where(head_of == r, dot(kept.astype(BF16), TV[:, at]), inner)
            Y[:, at] = inner

    def factor(j):
        return jnp.concatenate(
            [jnp.broadcast_to(jnp.exp(TOT[j][h : h + 1, :]), (HEAD_DIM, STATE)) for h in range(heads)],
            axis=0,
        )

    def mixer_gated():
        for k in range(1, n):
            links.arrived(end_slots[0][k], END.at[s ^ k], {"sp": s ^ k})
            links.arrived(end_slots[1][k], TOT.at[s ^ k], {"sp": s ^ k})
        state = jnp.zeros(END.shape[1:], F32)
        for j in range(n - 1):
            state = jnp.where(j < s, factor(j) * state + END[j].astype(F32), state)
        ENT[...] = state.astype(BF16)
        for g in range(groups):
            at = pl.ds(g * chan, chan)
            carried = dot(keys(RK, g), ENT[at, :], 1, 1)
            y = Y[:, at] + carried * LW[:, at]
            Y[:, at] = y
            gate = OGT[:, at].astype(F32)
            GB[pl.ds(0, tok), at] = (y * (gate * jax.nn.sigmoid(gate))).astype(BF16)
        if pieces == n:
            own = GB.at[pl.ds(0, tok), :]
            everyone(gated_slots, own, lambda k: GB.at[pl.ds(k * tok, tok), :])

    def mixer_states():
        for g in range(groups):
            at = pl.ds(g * chan, chan)
            gate = OGT[:, at].astype(F32)
            sig = jax.nn.sigmoid(gate)
            outer = OG[:, at] * (gate * sig)
            OB[:, at] = outer.astype(BF16)
            LED[:, at] = (outer * LW[:, at]).astype(BF16)
            BK[s, at, :] = dot(LED[:, at], keys(RK, g), 0, 0).astype(BF16)
        everyone(state_slots, BK.at[s], lambda k: BK.at[s])

    def mixer_scores():
        for g in range(groups):
            at = pl.ds(g * chan, chan)
            gate = OGT[:, at].astype(F32)
            sig = jax.nn.sigmoid(gate)
            DGT[:, at] = (OG[:, at] * Y[:, at] * sig * (1.0 + gate * (1.0 - sig))).astype(BF16)
            d_scores = jnp.zeros((tok, tok), F32)
            d_values = jnp.zeros((tok, chan), F32)
            for r in range(per_group):
                h = g * per_group + r
                one = jnp.where(head_of == r, OB[:, at].astype(F32), 0.0).astype(BF16)
                d_scores = d_scores + dot(one, TV[:, at], 1, 1) * DEC[h]
                d_values = jnp.where(head_of == r, dot(KT[h], OB[:, at]), d_values)
            OG[:, at] = d_values
            d_scores = d_scores.astype(BF16)
            ks = pl.ds(g * STATE, STATE)
            DRK[:, ks] = (dot(d_scores, keys(WK, g)) + dot(LED[:, at], ENT[at, :])).astype(BF16)
            DWF[:, ks] = dot(d_scores, keys(RK, g), 0, 0)

    def mixer_last():
        for k in range(1, n):
            links.arrived(state_slots[k], BK.at[s ^ k], {"sp": s ^ k})
        state = jnp.zeros(BK.shape[1:], F32)
        for j in range(n - 1, 0, -1):
            state = jnp.where(j > s, factor(j) * state + BK[j].astype(F32), state)
        leaving = state.astype(BF16)
        for g in range(groups):
            at = pl.ds(g * chan, chan)
            ks = pl.ds(g * STATE, STATE)
            mine_of = leaving[g * chan : (g + 1) * chan]
            DWK[:, ks] = (DWF[:, ks] + dot(TLD[:, at], mine_of)).astype(BF16)
            d_values = OG[:, at] + dot(keys(WK, g), mine_of, 1, 1) * TW[:, at]
            DV[:, at] = d_values.astype(BF16)

    order = [key for key in chunks]
    count = len(order)

    def forward(i):
        if i < count:
            p0(*order[i])
        if 0 <= i - 1 < count:
            chunks[order[i - 1]].p1()
        if 0 <= i - 2 < count:
            chunks[order[i - 2]].p2()

    def whole(q):
        for a in range(2):
            if (q, a) in chunks:
                chunks[(q, a)].p3()
        expert(q)
        portion(q)
        r0(q)

    mixer_ends()
    local_rows()
    for made in expert_loads:
        made.wait()
    if blocks == 4 and (0, 0) not in chunks:
        forward(0)
        expert(0)
        forward(1)
        portion(0)
        r0(0)
        forward(2)
        r1(0)
        mixer_inner()
        forward(3)
        r2(0)
        mixer_gated()
        forward(4)
        whole(1)
        r3(0)
        forward(5)
        r1(1)
        forward(6)
        whole(2)
        r2(1)
        forward(7)
        r1(2)
        r3(1)
        whole(3)
        r2(2)
        r1(3)
    else:
        mixer_inner()
        mixer_gated()
        for i in range(count + 2):
            forward(i)
        for q in range(blocks):
            whole(q)
        for q in range(blocks):
            r1(q)
        for q in range(blocks - 1):
            r2(q)
        for q in range(blocks - 2):
            r3(q)
    tiles = width // 256
    grads_gate_up(0, tiles // 4)
    r3(blocks - 2)
    r2(blocks - 1)
    grads_gate_up(tiles // 4, tiles // 2)
    r3(blocks - 1)
    grads_gate_up(tiles // 2, tiles)
    outs = [load(GW, gw_out), load(UW, uw_out)]
    for k in range(1, n):
        rows = pl.ds(k * cap, cap)
        links.arrived(back_slots[k], CB.at[rows, :], {"sp": s ^ k})

    half_tok = tok // 2
    gathers = []
    for i in range(2):

        def window(bits, part, i=i):
            row, rows = i * half_tok, half_tok
            if part is not None:
                row, rows = row + part * (half_tok // 2), half_tok // 2
            return G.at[:, pl.ds(row, rows), pl.ds(pl.multiple_of((t ^ bits) * pw, 128), pw)]

        gathers.append(Spread(links, t, window))
    here = pl.ds(pl.multiple_of(t * pw, 128), pw)
    back = dot(ONE[...], CB[...], 0, 0)
    for i in range(2):
        rows = pl.ds(i * half_tok, half_tok)
        for j in range(pieces):
            cot = C[rows, pl.ds(pl.multiple_of(j * strip + t * pw, 128), pw)].astype(F32)
            part = back[i * half_tok : (i + 1) * half_tok, j * pw : (j + 1) * pw]
            G[j, rows, here] = (cot + part).astype(BF16)
        gathers[i].p0()

    fars = []
    if pieces == n:
        far_slots = [links.slot() for _ in range(n)]
        for k in range(1, n):
            rows = pl.ds((k - 1) * tok, tok)
            links.start(far_slots[k], G.at[s ^ k, :, here], F.at[rows, here], {"sp": s ^ k})

            def window(bits, part, k=k):
                row, rows = (k - 1) * tok, tok
                if part is not None:
                    row, rows = row + part * half_tok, half_tok
                return F.at[pl.ds(row, rows), pl.ds(pl.multiple_of((t ^ bits) * pw, 128), pw)]

            fars.append(Spread(links, t, window))

    def far_p0(k):
        rows = pl.ds((k - 1) * tok, tok)
        links.arrived(far_slots[k], F.at[rows, here], {"sp": s ^ k})
        fars[k - 1].p0()

    grads_down()
    outs.append(load(DW, dw_out))
    for i in range(2):
        gathers[i].p1()
    for k in range(1, len(fars) + 1):
        far_p0(k)
    for i in range(2):
        gathers[i].p2()
    for i in range(2):
        gathers[i].p3()
    proj_load.wait()
    OG[...] = sum(dot(G[j], OP[pl.ds(j * strip, strip), :]) for j in range(pieces))
    mixer_states()
    for far in fars:
        far.p1()
    mixer_scores()
    outs.append(load(DGT, gate_out))
    outs.append(load(DRK, read_out))
    for far in fars:
        far.p2()

    def proj_own(i, _):
        at = pl.ds(pl.multiple_of(i * 256, 128), 256)
        PJ[at, :] = dot(G[s, :, at], GB[pl.ds(0, tok), :], 0, 0)
        return 0

    def proj_far(i, _):
        at = pl.ds(pl.multiple_of(i * 256, 128), 256)
        PJ[at, :] += dot(F[:, at], GB[pl.ds(tok, (n - 1) * tok), :], 0, 0)
        return 0

    if pieces == n:
        lax.fori_loop(0, strip // 256, proj_own, 0)
    mixer_last()
    outs.append(load(DWK, write_out))
    outs.append(load(DV, value_out))
    if pieces == n:
        for far in fars:
            far.p3()
        for k in range(1, n):
            links.arrived(gated_slots[k], GB.at[pl.ds(k * tok, tok), :], {"sp": s ^ k})
        lax.fori_loop(0, strip // 256, proj_far, 0)
        outs.append(load(PJ, outs_proj[0]))
    else:
        for j in range(pieces):
            outs.append(load(G.at[j], outs_proj[0].at[:, pl.ds(j * strip, strip)]))
        outs.append(load(GB.at[pl.ds(0, tok), :], outs_proj[1]))
    links.finish()
    for made in outs:
        made.wait()


def body(
    token_values,
    write_keys,
    read_keys,
    log_decay,
    out_gate,
    out_proj,
    mixed,
    cotangent,
    route_ids,
    route_weights,
    w_gate,
    w_up,
    w_down,
):
    tok, width = mixed.shape
    n = lax.axis_size("sp")
    ranks = lax.axis_size("tp")
    hid = w_gate.shape[2]
    inner = token_values.shape[1]
    heads = log_decay.shape[0]
    share = width // ranks
    cap = 3 * tok // n
    rows = n * cap
    pieces = n if (width // n // ranks) % 128 == 0 else 1
    far = pieces == n
    strip = width // pieces
    blocks = 4 if n % 4 == 0 else n
    R = rows // blocks
    slots = 2 * n + 2 * blocks * 9 + 5 * blocks + 6 * n + 18 + 9 * n
    any_ = pl.BlockSpec(memory_space=pl.ANY)

    def buf(*shape, dtype=BF16):
        return pltpu.VMEM(shape, dtype)

    def like(a):
        return jax.ShapeDtypeStruct(a.shape, a.dtype)

    if far:
        proj_shapes = [jax.ShapeDtypeStruct((strip, inner), F32)]
    else:
        proj_shapes = [jax.ShapeDtypeStruct((tok, width), BF16), jax.ShapeDtypeStruct((tok, inner), BF16)]
    operands = [
        route_ids.T,
        route_weights.T,
        mixed,
        cotangent,
        w_gate[0],
        w_up[0],
        w_down[0],
        token_values,
        write_keys,
        read_keys,
        log_decay,
        out_gate,
        out_proj,
    ]
    outputs = (
        [like(token_values), like(write_keys), like(read_keys), like(out_gate)]
        + proj_shapes
        + [like(w_gate[0]), like(w_up[0]), like(w_down[0])]
    )
    got = pl.pallas_call(
        functools.partial(main_kernel, n, ranks, pieces),
        out_shape=outputs,
        in_specs=[any_] * len(operands),
        out_specs=[any_] * len(outputs),
        scratch_shapes=[
            buf(*route_ids.T.shape, dtype=jnp.int32),
            buf(*route_ids.T.shape, dtype=F32),
            buf(tok, width),
            buf(tok, width),
            buf(width, 2 * hid),
            buf(hid, width),
            buf(rows, width),
            buf(rows, width),
            buf(n - 1, cap, share),
            buf(n - 1, cap, share),
            buf(rows, tok),
            buf(cap, 128, dtype=F32),
            buf(rows, 2 * hid),
            buf(rows, hid),
            buf(hid, rows),
            buf(blocks, 2, 2, ranks // 4, R, share),
            buf(blocks, 2, ranks // 4, R, share),
            buf(blocks, 2, R, share // 2),
            buf(blocks, 2, R, share // 2),
            buf(blocks, R, share // 2),
            buf(blocks, R, share // 2),
            buf(rows, share),
            buf(rows, share),
            buf(pieces, tok, strip),
            buf(width, hid),
            buf(width, hid),
            buf(hid, width),
            buf(*token_values.shape),
            buf(*write_keys.shape),
            buf(*read_keys.shape),
            buf(*log_decay.shape, dtype=F32),
            buf(*out_gate.shape),
            buf(*out_proj.shape),
            buf(tok, inner, dtype=F32),
            buf(tok, inner, dtype=F32),
            buf(tok, inner, dtype=F32),
            buf(heads, tok, tok, dtype=F32),
            buf(heads, tok, tok),
            buf(tok, inner),
            buf(n, inner, STATE),
            buf(n, max(heads, 8), STATE, dtype=F32),
            buf(n, inner, STATE),
            buf(inner, STATE),
            buf(n * tok if far else tok, inner),
            buf((n - 1) * tok if far else 16, strip if far else 128),
            buf(tok, inner, dtype=F32),
            buf(tok, inner),
            buf(tok, inner),
            buf(*write_keys.shape, dtype=F32),
            buf(tok, inner),
            buf(*write_keys.shape),
            buf(*read_keys.shape),
            buf(tok, inner),
            buf(*((strip, inner) if far else (8, 128)), dtype=F32),
            pltpu.SemaphoreType.DMA((slots,)),
            pltpu.SemaphoreType.DMA((slots,)),
            pltpu.SemaphoreType.DMA((24 + pieces,)),
        ],
        compiler_params=pltpu.CompilerParams(
            collective_id=1, has_side_effects=True, vmem_limit_bytes=60 * 1024 * 1024
        ),
    )(*operands)
    value_grad, write_grad, read_grad, gate_grad = got[:4]
    grad_gate, grad_up, grad_down = got[-3:]
    if far:
        proj_grad = got[4]
    else:
        proj_part = dot(got[4], got[5], 0, 0).astype(BF16)
        proj_grad = lax.psum_scatter(proj_part, "sp", scatter_dimension=0, tiled=True).astype(F32)
    return (
        value_grad,
        write_grad,
        read_grad,
        gate_grad,
        proj_grad,
        grad_gate[None],
        grad_up[None],
        grad_down[None],
    )


def solution(mesh):
    return jax.shard_map(
        body,
        mesh=mesh,
        in_specs=(
            P("sp", "tp"),
            P("sp", "tp"),
            P("sp", "tp"),
            P("tp", "sp"),
            P("sp", "tp"),
            P(None, "tp"),
            P("sp", None),
            P("sp", None),
            P("sp", None),
            P("sp", None),
            P("sp", None, "tp"),
            P("sp", None, "tp"),
            P("sp", "tp", None),
        ),
        out_specs=(
            P("sp", "tp"),
            P("sp", "tp"),
            P("sp", "tp"),
            P("sp", "tp"),
            P("sp", "tp"),
            P("sp", None, "tp"),
            P("sp", None, "tp"),
            P("sp", "tp", None),
        ),
        check_vma=False,
    )
```

time: 212 us -> 143 us (0.67)
  matrix products: 28.9 us -> 0 us
  starting transfers between devices: 17.1 us -> 0 us
  other arithmetic: 11.2 us -> 0 us
  Pallas kernels: 132 us -> 127 us
  local copies, waits for them, and re-layouts: 18.8 us -> 14.5 us
  waiting for transfers between devices: 2.14 us -> 0 us
    dot_general x25 -> x0, matrix products: 28.9 us -> none  [dot(): lax.dot_general(a, b, (((ca,), (cb,)), ((), ())), preferred_element_type=...]
    ppermute x11 -> x0, starting transfers between devices: 17.1 us -> none  [shift(): return lax.ppermute(x, 'sp', [(i, (i + by) % n) for i in range(n)])]
    pallas_call x2 -> x1, Pallas kernels: 132 us -> 127 us  [body(): pl.pallas_call(functools.partial(main_kernel, n, ranks, pieces), out_shap...]
    unnamed x55 -> x14, local copies, waits for them, and re-layouts: 11 us -> 14.5 us
    convert_element_type x5 -> x0, other arithmetic: 2.91 us -> none  [the longest x2 1.83 us: body(): got = shift(packed, j).astype(F32)]
    another operation x5 -> x0, other arithmetic: 2.74 us -> none
    eq x4 -> x0, local copies, waits for them, and re-layouts: 2.45 us -> none  [body(): chosen = slot[:, None, :] == place[None, :, None]]
    ppermute x11 -> x0, waiting for transfers between devices: 2.14 us -> none  [shift(): return lax.ppermute(x, 'sp', [(i, (i + by) % n) for i in range(n)])]
  transfers between devices with their start and end apart: 11 -> 0, of which waited for: 1 -> 0; matrix products, arithmetic and copies ran while one was open for 16% -> 0% of each run, Pallas kernels for 63% -> 0%
where the time goes in v2:
time: 143 us; the launch traced here: 142 us
  Pallas kernels  127 us (89%)
  local copies, waits for them, and re-layouts  14.5 us (10%)
    pallas_call x1, Pallas kernels, body(): pl.pallas_call(functools.partial(main_kernel, n, ranks, pieces), out_shap...  127 us
    unnamed x14, local copies, waits for them, and re-layouts  14.5 us

profile of v2, /device:TPU:0, one launch (start us, length us, event | category | flops | bytes accessed | tf_op | source)
XLA Modules:
  0.0 141.9 jit_solution(14293347413953337142)
XLA Ops:
  0.6 126.7 %shard_map.188 = (bf16[256,256]{1,0:T(8,128)(2,1)}, bf16[256,128]{1,0:T(8,128)(2,1)}, bf16[256,128]{1,0:T(8,128)(2,1)}, bf16[256,256]{1,0:T(8,128)(2,1)}, f32[10...) custom-call(s32[2,256]{1,0:T(2,128)} %bitcast.14, ...), custom_call_target="tpu_custom_call" | custom-call | tf_op jit(solution)/shard_map/pallas_call | solution.py:693
  127.4 0.0 copy-start.2
  127.4 1.7 %copy.29 = bf16[256,256]{1,0:T(8,128)(2,1)} copy(bf16[256,256]{1,0:T(8,128)(2,1)} %get-tuple-element.32) | data formatting | bytes 262144
  129.1 1.5 %copy.30 = bf16[256,128]{1,0:T(8,128)(2,1)} copy(bf16[256,128]{1,0:T(8,128)(2,1)} %get-tuple-element.33) | data formatting | bytes 131072
  130.6 1.5 %copy.31 = bf16[256,128]{1,0:T(8,128)(2,1)} copy(bf16[256,128]{1,0:T(8,128)(2,1)} %get-tuple-element.34) | data formatting | bytes 131072
  132.1 1.6 %copy.32 = bf16[256,256]{1,0:T(8,128)(2,1)} copy(bf16[256,256]{1,0:T(8,128)(2,1)} %get-tuple-element.35) | data formatting | bytes 262144
  133.6 2.3 %copy.33 = f32[1024,256]{1,0:T(8,128)} copy(f32[1024,256]{1,0:T(8,128)} %get-tuple-element.36) | data formatting | bytes 2097152
  135.9 0.0 copy-done.2
  135.9 0.0 copy-start.1
  135.9 1.3 copy.34
  137.2 1.0 copy-done.1
  138.2 0.0 copy-start
  138.2 1.3 copy.35
  139.6 1.0 copy-done
  140.6 1.3 copy.36
Async XLA Ops:
  127.4 8.5 %copy-start.2 = (bf16[4096,256]{1,0:T(8,128)(2,1)S(1)}, bf16[4096,256]{1,0:T(8,128)(2,1)}, u32[]{:S(2)}) copy-start(bf16[4096,256]{1,0:T(8,128)(2,1)} %get-tuple-element.21) | copy-start | bytes 6291460
  135.9 2.3 %copy-start.1 = (bf16[4096,256]{1,0:T(8,128)(2,1)S(1)}, bf16[4096,256]{1,0:T(8,128)(2,1)}, u32[]{:S(2)}) copy-start(bf16[4096,256]{1,0:T(8,128)(2,1)} %get-tuple-element.22) | copy-start | bytes 6291460
  138.2 2.3 %copy-start = (bf16[256,4096]{1,0:T(8,128)(2,1)S(1)}, bf16[256,4096]{1,0:T(8,128)(2,1)}, u32[]{:S(2)}) copy-start(bf16[256,4096]{1,0:T(8,128)(2,1)} %get-tuple-element.23) | copy-start | bytes 6291460

commit v3 on v2

--- a/solution.py
+++ b/solution.py
@@ -13,6 +13,7 @@
 F32 = jnp.float32
 BF16 = jnp.bfloat16
 MESH = pl.DeviceIdType.MESH
+VMEM_LIMIT = 54 * 1024 * 1024
 
 
 def dot(a, b, ca=1, cb=0):
@@ -113,21 +114,24 @@
     decay_in,
     gate_in,
     proj_in,
-    value_out,
-    write_out,
-    read_out,
-    gate_out,
+    DV,
+    DWK,
+    DRK,
+    DGT,
+    GW,
+    UW,
+    DW,
     *refs,
 ):
     outs_proj = refs[: 1 if pieces == n else 2]
-    gw_out, uw_out, dw_out = refs[len(outs_proj) : len(outs_proj) + 3]
     (
         IDS, RW, M, C, W2, WD, X, S, SX, SS, ONE, WCOL, DGU, HID, HT,
-        PB, RB, RX, RY, RX2, RY2, FIN, CB, G, GW, UW, DW,
+        PB, RB, RX, RY, RX2, RY2, FIN, CB, G,
         TV, WK, RK, LD, OGT, OP, LW, TW, Y, DEC, KT, TLD, END, TOT, BK, ENT, GB, F,
-        OG, OB, LED, DWF, DV, DWK, DRK, DGT, PJ,
+        OG, OB, LED, DWF, MP, CP, ACT, DFAC, BACK,
         send_sem, recv_sem, local_sem,
-    ) = refs[len(outs_proj) + 3 :]
+    ) = refs[len(outs_proj) :]
+    PJ = outs_proj[0]
     t = lax.axis_index("tp")
     s = lax.axis_index("sp")
     tok, width = M.shape
@@ -157,7 +161,14 @@
         made.start()
         return made
 
-    first_loads = [load(ids_in, IDS), load(weights_in, RW), load(mixed, M), load(cotangent, C)]
+    mine = pl.ds(pl.multiple_of(t * share, 128), share)
+    first_loads = [
+        load(ids_in, IDS),
+        load(weights_in, RW),
+        load(mixed.at[:, mine], MP),
+        load(cotangent.at[:, mine], CP),
+    ]
+    row_loads = [load(mixed, M), load(cotangent, C)]
     mix_loads = [
         load(decay_in, LD),
         load(writes_in, WK),
@@ -187,9 +198,8 @@
     slot = jnp.where(member, slot, -1.0).astype(jnp.int32)
     place = lax.broadcasted_iota(jnp.int32, (cap, tok), 0)
 
-    mine = pl.ds(pl.multiple_of(t * share, 128), share)
     z_slots = [[links.slot() for _ in range(n)] for _ in range(2)]
-    m_part, c_part = M[:, mine], C[:, mine]
+    m_part, c_part = MP[...], CP[...]
     for k in list(range(1, n)) + [0]:
         rows = pl.ds(k * cap, cap)
         chosen = slot[k : k + 1, :] == place
@@ -205,6 +215,9 @@
             WCOL[...] = jnp.broadcast_to(row_weight, WCOL.shape)
 
     def local_rows():
+        for made in row_loads:
+            made.wait()
+
         def some(i, _):
             at = pl.ds(pl.multiple_of(i * share, 128), share)
             pick = ONE[pl.ds(0, cap), :]
@@ -236,16 +249,21 @@
                 links.arrived(z_slots[a][k], ref.at[pl.ds(k * cap, cap), mine], {"sp": s ^ k})
         chunks[(q, a)].p0()
 
-    def expert(q):
+    def expert_a(q):
         r = pl.ds(q * R, R)
         both = dot(X[r, :], W2[...])
         gate, up = both[:, :hid], both[:, hid:]
         sigma = jax.nn.sigmoid(gate)
         act = gate * sigma
         HID[r, :] = (act * up).astype(BF16)
+        ACT[...] = act
+        DFAC[...] = up * sigma * (1.0 + gate * (1.0 - sigma))
+
+    def expert_b(q):
+        r = pl.ds(q * R, R)
         d_act = dot(S[r, :], WD[...], 1, 1)
-        DGU[r, pl.ds(0, hid)] = (d_act * up * sigma * (1.0 + gate * (1.0 - sigma))).astype(BF16)
-        DGU[r, pl.ds(hid, hid)] = (d_act * act).astype(BF16)
+        DGU[r, pl.ds(0, hid)] = (d_act * DFAC[...]).astype(BF16)
+        DGU[r, pl.ds(hid, hid)] = (d_act * ACT[...]).astype(BF16)
 
     def portion(q):
         r = pl.ds(q * R, R)
@@ -472,88 +490,108 @@
         if 0 <= i - 2 < count:
             chunks[order[i - 2]].p2()
 
-    def whole(q):
-        for a in range(2):
-            if (q, a) in chunks:
-                chunks[(q, a)].p3()
-        expert(q)
+    def landed(q, a):
+        if (q, a) in chunks:
+            chunks[(q, a)].p3()
+
+    def rest(q):
+        landed(q, 1)
+        expert_b(q)
         portion(q)
         r0(q)
 
+    def add_back(first, last, start):
+        rows = pl.ds(first * cap, (last - first) * cap)
+        for k in range(max(first, 1), last):
+            one = pl.ds(k * cap, cap)
+            links.arrived(back_slots[k], CB.at[one, :], {"sp": s ^ k})
+        part = dot(ONE[rows, :], CB[rows, :], 0, 0)
+        BACK[...] = part if start else BACK[...] + part
+
+    tiles = width // 256
     mixer_ends()
-    local_rows()
-    for made in expert_loads:
-        made.wait()
     if blocks == 4 and (0, 0) not in chunks:
         forward(0)
-        expert(0)
+        local_rows()
+        for made in expert_loads:
+            made.wait()
         forward(1)
+        expert_a(0)
+        expert_b(0)
+        forward(2)
         portion(0)
         r0(0)
-        forward(2)
-        r1(0)
+        forward(3)
         mixer_inner()
-        forward(3)
-        r2(0)
-        mixer_gated()
+        landed(1, 0)
+        expert_a(1)
         forward(4)
-        whole(1)
-        r3(0)
+        rest(1)
         forward(5)
         r1(1)
+        mixer_gated()
+        landed(2, 0)
+        expert_a(2)
         forward(6)
-        whole(2)
+        rest(2)
+        forward(7)
         r2(1)
-        forward(7)
         r1(2)
+        landed(3, 0)
+        expert_a(3)
         r3(1)
-        whole(3)
+        rest(3)
         r2(2)
         r1(3)
+        r1(0)
+        grads_gate_up(0, tiles // 8)
+        r3(2)
+        r2(3)
+        grads_gate_up(tiles // 8, tiles // 4)
+        r2(0)
+        r3(3)
+        grads_gate_up(tiles // 4, tiles // 2)
+        add_back(1, 3, True)
+        r3(0)
+        add_back(0, 1, False)
+        add_back(3, 4, False)
     else:
+        local_rows()
+        for made in expert_loads:
+            made.wait()
         mixer_inner()
         mixer_gated()
         for i in range(count + 2):
             forward(i)
         for q in range(blocks):
-            whole(q)
-        for q in range(blocks):
-            r1(q)
-        for q in range(blocks - 1):
-            r2(q)
-        for q in range(blocks - 2):
-            r3(q)
-    tiles = width // 256
-    grads_gate_up(0, tiles // 4)
-    r3(blocks - 2)
-    r2(blocks - 1)
-    grads_gate_up(tiles // 4, tiles // 2)
-    r3(blocks - 1)
-    grads_gate_up(tiles // 2, tiles)
-    outs = [load(GW, gw_out), load(UW, uw_out)]
-    for k in range(1, n):
-        rows = pl.ds(k * cap, cap)
-        links.arrived(back_slots[k], CB.at[rows, :], {"sp": s ^ k})
+            landed(q, 0)
+            expert_a(q)
+            rest(q)
+        for stage in (r1, r2, r3):
+            for q in range(blocks):
+                stage(q)
+        grads_gate_up(0, tiles // 2)
+        add_back(0, n, True)
 
     half_tok = tok // 2
+    cuts = 4
+    cut = tok // cuts
     gathers = []
-    for i in range(2):
+    for i in range(cuts):
 
         def window(bits, part, i=i):
-            row, rows = i * half_tok, half_tok
+            row, rows = i * cut, cut
             if part is not None:
-                row, rows = row + part * (half_tok // 2), half_tok // 2
+                row, rows = row + part * (cut // 2), cut // 2
             return G.at[:, pl.ds(row, rows), pl.ds(pl.multiple_of((t ^ bits) * pw, 128), pw)]
 
         gathers.append(Spread(links, t, window))
     here = pl.ds(pl.multiple_of(t * pw, 128), pw)
-    back = dot(ONE[...], CB[...], 0, 0)
-    for i in range(2):
-        rows = pl.ds(i * half_tok, half_tok)
+    for i in range(cuts):
+        rows = pl.ds(i * cut, cut)
         for j in range(pieces):
             cot = C[rows, pl.ds(pl.multiple_of(j * strip + t * pw, 128), pw)].astype(F32)
-            part = back[i * half_tok : (i + 1) * half_tok, j * pw : (j + 1) * pw]
-            G[j, rows, here] = (cot + part).astype(BF16)
+            G[j, rows, here] = (cot + BACK[rows, pl.ds(j * pw, pw)]).astype(BF16)
         gathers[i].p0()
 
     fars = []
@@ -577,55 +615,70 @@
         fars[k - 1].p0()
 
     grads_down()
-    outs.append(load(DW, dw_out))
-    for i in range(2):
+    for i in range(cuts):
         gathers[i].p1()
+        if i:
+            gathers[i - 1].p2()
+    gathers[cuts - 1].p2()
     for k in range(1, len(fars) + 1):
         far_p0(k)
-    for i in range(2):
-        gathers[i].p2()
-    for i in range(2):
+    for i in range(cuts):
         gathers[i].p3()
     proj_load.wait()
     OG[...] = sum(dot(G[j], OP[pl.ds(j * strip, strip), :]) for j in range(pieces))
+    def proj_own(i, _):
+        at = pl.ds(pl.multiple_of(i * 256, 128), 256)
+        PJ[at, :] = dot(G[s, :, at], GB[pl.ds(0, tok), :], 0, 0)
+        return 0
+
+    def proj_far(i, _):
+        at = pl.ds(pl.multiple_of(i * 256, 128), 256)
+        PJ[at, :] += dot(F[:, at], GB[pl.ds(tok, (n - 1) * tok), :], 0, 0)
+        return 0
+
     mixer_states()
     for far in fars:
         far.p1()
     mixer_scores()
-    outs.append(load(DGT, gate_out))
-    outs.append(load(DRK, read_out))
     for far in fars:
         far.p2()
-
-    def proj_own(i, _):
-        at = pl.ds(pl.multiple_of(i * 256, 128), 256)
-        PJ[at, :] = dot(G[s, :, at], GB[pl.ds(0, tok), :], 0, 0)
-        return 0
-
-    def proj_far(i, _):
-        at = pl.ds(pl.multiple_of(i * 256, 128), 256)
-        PJ[at, :] += dot(F[:, at], GB[pl.ds(tok, (n - 1) * tok), :], 0, 0)
-        return 0
-
     if pieces == n:
         lax.fori_loop(0, strip // 256, proj_own, 0)
+    grads_gate_up(tiles // 2, tiles)
     mixer_last()
-    outs.append(load(DWK, write_out))
-    outs.append(load(DV, value_out))
     if pieces == n:
         for far in fars:
             far.p3()
         for k in range(1, n):
             links.arrived(gated_slots[k], GB.at[pl.ds(k * tok, tok), :], {"sp": s ^ k})
         lax.fori_loop(0, strip // 256, proj_far, 0)
-        outs.append(load(PJ, outs_proj[0]))
     else:
         for j in range(pieces):
-            outs.append(load(G.at[j], outs_proj[0].at[:, pl.ds(j * strip, strip)]))
-        outs.append(load(GB.at[pl.ds(0, tok), :], outs_proj[1]))
+            outs_proj[0][:, pl.ds(j * strip, strip)] = G[j]
+        outs_proj[1][...] = GB[pl.ds(0, tok), :]
     links.finish()
-    for made in outs:
-        made.wait()
+
+
+def place_kernel(count, *refs):
+    sources, places, sem = refs[:count], refs[count : 2 * count], refs[-1]
+    made = [pltpu.make_async_copy(sources[i], places[i], sem.at[i]) for i in range(count)]
+    for one in made:
+        one.start()
+    for one in made:
+        one.wait()
+
+
+def place(arrays):
+    any_ = pl.BlockSpec(memory_space=pl.ANY)
+    count = len(arrays)
+    return pl.pallas_call(
+        functools.partial(place_kernel, count),
+        out_shape=[jax.ShapeDtypeStruct(a.shape, a.dtype) for a in arrays],
+        in_specs=[any_] * count,
+        out_specs=[any_] * count,
+        scratch_shapes=[pltpu.SemaphoreType.DMA((count,))],
+        compiler_params=pltpu.CompilerParams(vmem_limit_bytes=1024 * 1024),
+    )(*arrays)
 
 
 def body(
@@ -664,12 +717,12 @@
         return pltpu.VMEM(shape, dtype)
 
     def like(a):
-        return jax.ShapeDtypeStruct(a.shape, a.dtype)
+        return pltpu.VMEM(a.shape, a.dtype)
 
     if far:
-        proj_shapes = [jax.ShapeDtypeStruct((strip, inner), F32)]
+        proj_shapes = [pltpu.VMEM((strip, inner), F32)]
     else:
-        proj_shapes = [jax.ShapeDtypeStruct((tok, width), BF16), jax.ShapeDtypeStruct((tok, inner), BF16)]
+        proj_shapes = [pltpu.VMEM((tok, width), BF16), pltpu.VMEM((tok, inner), BF16)]
     operands = [
         route_ids.T,
         route_weights.T,
@@ -687,14 +740,14 @@
     ]
     outputs = (
         [like(token_values), like(write_keys), like(read_keys), like(out_gate)]
+        + [like(w_gate[0]), like(w_up[0]), like(w_down[0])]
         + proj_shapes
-        + [like(w_gate[0]), like(w_up[0]), like(w_down[0])]
     )
     got = pl.pallas_call(
         functools.partial(main_kernel, n, ranks, pieces),
         out_shape=outputs,
         in_specs=[any_] * len(operands),
-        out_specs=[any_] * len(outputs),
+        out_specs=[pl.BlockSpec(memory_space=pltpu.VMEM)] * len(outputs),
         scratch_shapes=[
             buf(*route_ids.T.shape, dtype=jnp.int32),
             buf(*route_ids.T.shape, dtype=F32),
@@ -720,9 +773,6 @@
             buf(rows, share),
             buf(rows, share),
             buf(pieces, tok, strip),
-            buf(width, hid),
-            buf(width, hid),
-            buf(hid, width),
             buf(*token_values.shape),
             buf(*write_keys.shape),
             buf(*read_keys.shape),
@@ -745,25 +795,25 @@
             buf(tok, inner),
             buf(tok, inner),
             buf(*write_keys.shape, dtype=F32),
-            buf(tok, inner),
-            buf(*write_keys.shape),
-            buf(*read_keys.shape),
-            buf(tok, inner),
-            buf(*((strip, inner) if far else (8, 128)), dtype=F32),
+            buf(tok, share),
+            buf(tok, share),
+            buf(R, hid, dtype=F32),
+            buf(R, hid, dtype=F32),
+            buf(tok, share, dtype=F32),
             pltpu.SemaphoreType.DMA((slots,)),
             pltpu.SemaphoreType.DMA((slots,)),
             pltpu.SemaphoreType.DMA((24 + pieces,)),
         ],
         compiler_params=pltpu.CompilerParams(
-            collective_id=1, has_side_effects=True, vmem_limit_bytes=60 * 1024 * 1024
+            collective_id=1, has_side_effects=True, vmem_limit_bytes=VMEM_LIMIT
         ),
     )(*operands)
-    value_grad, write_grad, read_grad, gate_grad = got[:4]
-    grad_gate, grad_up, grad_down = got[-3:]
+    placed = place(got if far else got[:7])
+    value_grad, write_grad, read_grad, gate_grad, grad_gate, grad_up, grad_down = placed[:7]
     if far:
-        proj_grad = got[4]
+        proj_grad = placed[7]
     else:
-        proj_part = dot(got[4], got[5], 0, 0).astype(BF16)
+        proj_part = dot(got[7], got[8], 0, 0).astype(BF16)
         proj_grad = lax.psum_scatter(proj_part, "sp", scatter_dimension=0, tiled=True).astype(F32)
     return (
         value_grad,

time: 143 us -> 127 us (0.89)
  local copies, waits for them, and re-layouts: 14.5 us -> 0 us
    unnamed x14 -> x0, local copies, waits for them, and re-layouts: 14.5 us -> none
    pallas_call x1, Pallas kernels: 127 us -> 123 us  [body(): pl.pallas_call(functools.partial(main_kernel, n, ranks, pieces), out_shap...]
    pallas_call x0 -> x1, Pallas kernels: none -> 3.18 us  [place(): pl.pallas_call(functools.partial(place_kernel, count), out_shape=[jax.Sha...]
where the time goes in v3:
time: 127 us
  Pallas kernels  126 us (99%)
    pallas_call x1, Pallas kernels, body(): pl.pallas_call(functools.partial(main_kernel, n, ranks, pieces), out_shap...  123 us
    pallas_call x1, Pallas kernels, place(): pl.pallas_call(functools.partial(place_kernel, count), out_shape=[jax.Sha...  3.18 us

profile of v3, /device:TPU:0, one launch (start us, length us, event | category | flops | bytes accessed | tf_op | source)
XLA Modules:
  0.0 126.8 jit_solution(14760436252576082933)
XLA Ops:
  0.6 122.9 %shard_map.188 = (bf16[256,256]{1,0:T(8,128)(2,1)S(1)}, bf16[256,128]{1,0:T(8,128)(2,1)S(1)}, bf16[256,128]{1,0:T(8,128)(2,1)S(1)}, bf16[256,256]{1,0:T(8,128)(2...) custom-call(s32[2,256]{1,0:T(2,128)} %bitcast.11, ...), custom_call_target="tpu_custom_call" | custom-call | tf_op jit(solution)/shard_map/pallas_call | solution.py:746
  123.6 3.2 %shard_map.189 = (bf16[256,256]{1,0:T(8,128)(2,1)}, bf16[256,128]{1,0:T(8,128)(2,1)}, bf16[256,128]{1,0:T(8,128)(2,1)}, bf16[256,256]{1,0:T(8,128)(2,1)}, bf16[4...) custom-call(bf16[256,256]{1,0:T(8,128)(2,1)S(1)} %get-tuple-element.24.refs_0_, ...), custom_call_target="tpu_custom_call" | custom-call | tf_op jit(solution)/shard_map/pallas_call | solution.py:674

commit v4 on v3

--- a/solution.py
+++ b/solution.py
@@ -168,6 +168,9 @@
         load(mixed.at[:, mine], MP),
         load(cotangent.at[:, mine], CP),
     ]
+    greet(n, t, s)
+    for made in first_loads:
+        made.wait()
     row_loads = [load(mixed, M), load(cotangent, C)]
     mix_loads = [
         load(decay_in, LD),
@@ -182,9 +185,6 @@
         load(w_down, WD),
     ]
     proj_load = load(proj_in, OP)
-    greet(n, t, s)
-    for made in first_loads:
-        made.wait()
 
     rows_n = max(n, 8)
     lane = lax.broadcasted_iota(jnp.int32, (rows_n, tok), 0) ^ s
@@ -539,8 +539,8 @@
         r1(2)
         landed(3, 0)
         expert_a(3)
+        rest(3)
         r3(1)
-        rest(3)
         r2(2)
         r1(3)
         r1(0)
@@ -550,7 +550,7 @@
         grads_gate_up(tiles // 8, tiles // 4)
         r2(0)
         r3(3)
-        grads_gate_up(tiles // 4, tiles // 2)
+        grads_gate_up(tiles // 4, tiles)
         add_back(1, 3, True)
         r3(0)
         add_back(0, 1, False)
@@ -574,7 +574,7 @@
         add_back(0, n, True)
 
     half_tok = tok // 2
-    cuts = 4
+    cuts = 2
     cut = tok // cuts
     gathers = []
     for i in range(cuts):
@@ -644,7 +644,6 @@
         far.p2()
     if pieces == n:
         lax.fori_loop(0, strip // 256, proj_own, 0)
-    grads_gate_up(tiles // 2, tiles)
     mixer_last()
     if pieces == n:
         for far in fars:

time: 127 us -> 122 us (0.961)
  Pallas kernels: 126 us -> 121 us
    pallas_call x1, Pallas kernels: 123 us -> 118 us  [body(): pl.pallas_call(functools.partial(main_kernel, n, ranks, pieces), out_shap...]
where the time goes in v4:
time: 122 us
  Pallas kernels  121 us (99%)
    pallas_call x1, Pallas kernels, body(): pl.pallas_call(functools.partial(main_kernel, n, ranks, pieces), out_shap...  118 us
    pallas_call x1, Pallas kernels, place(): pl.pallas_call(functools.partial(place_kernel, count), out_shape=[jax.Sha...  3.18 us

profile of v4, /device:TPU:0, one launch (start us, length us, event | category | flops | bytes accessed | tf_op | source)
XLA Modules:
  0.0 122.0 jit_solution(4039928702344710113)
XLA Ops:
  0.6 118.1 %shard_map.188 = (bf16[256,256]{1,0:T(8,128)(2,1)S(1)}, bf16[256,128]{1,0:T(8,128)(2,1)S(1)}, bf16[256,128]{1,0:T(8,128)(2,1)S(1)}, bf16[256,256]{1,0:T(8,128)(2...) custom-call(s32[2,256]{1,0:T(2,128)} %bitcast.11, ...), custom_call_target="tpu_custom_call" | custom-call | tf_op jit(solution)/shard_map/pallas_call | solution.py:745
  118.8 3.2 %shard_map.189 = (bf16[256,256]{1,0:T(8,128)(2,1)}, bf16[256,128]{1,0:T(8,128)(2,1)}, bf16[256,128]{1,0:T(8,128)(2,1)}, bf16[256,256]{1,0:T(8,128)(2,1)}, bf16[4...) custom-call(bf16[256,256]{1,0:T(8,128)(2,1)S(1)} %get-tuple-element.24.refs_0_, ...), custom_call_target="tpu_custom_call" | custom-call | tf_op jit(solution)/shard_map/pallas_call | solution.py:673
